TPU v7x, 32 devices: a whole 2x2x4 slice. The times are simulated.
32 devices in a mesh: sp: 8 (over z, x), tp: 4 (over y, core).
Axes of the slice: x: 2, y: 2, z: 4, core: 2. Of those that a mesh axis runs over, the one named last changes fastest.
Arguments:
- target_rows: bfloat16 [512, 2048], P(('sp', 'tp')), may hold values from -6 to 6
- source_rows: bfloat16 [2048, 2048], P(('sp', 'tp')), may hold values from -6 to 6
- norm_gain: bfloat16 [2048], replicated, may hold values from 0.099609375 to 1.8984375
- query_weight: bfloat16 [2048, 4096], P(None, 'tp'), may hold values from -0.125 to 0.125
- key_weight: bfloat16 [2048, 4096], P(None, 'tp'), may hold values from -0.125 to 0.125
- value_weight: bfloat16 [2048, 4096], P(None, 'tp'), may hold values from -0.125 to 0.125
- output_weight: bfloat16 [4096, 2048], P('tp'), may hold values from -0.09375 to 0.09375
- saved_output: bfloat16 [512, 4096], P('sp', 'tp'), may hold values from -3 to 3
- norm_offset: bfloat16 [512, 16], P('sp', 'tp'), may hold values from 0.25 to 1.25
- output_grad: bfloat16 [512, 2048], P(('sp', 'tp')), may hold values from -192 to 192
Outputs:
- target_grad: float32 [512, 2048], P(('sp', 'tp'))
- source_grad: float32 [2048, 2048], P(('sp', 'tp'))
- query_weight_grad: float32 [2048, 4096], P('sp', 'tp')
All inputs are finite; a program needn't handle non-finite values.
Results may differ from a plain program's by a relative error of at most 0.033.
Values may be sent and summed in bfloat16 or wider, within the bound.
A program may use at most 64 MiB of HBM per device.

v0:
```python
import functools
import math

import jax
import jax.numpy as jnp
from jax import lax
from jax.experimental import pallas as pl
from jax.experimental.pallas import tpu as pltpu
from jax.sharding import PartitionSpec as P

HEAD_DIM = 256
EPSILON = 1e-06
MESH = pl.DeviceIdType.MESH
BF = jnp.bfloat16
F32 = jnp.float32
VMEM = pl.BlockSpec(memory_space=pltpu.VMEM)


def contract_last(left, right):
    return lax.dot_general(left, right, (((1,), (1,)), ((), ())), preferred_element_type=F32)


def push(src, dst, send, recv, device):
    return pltpu.make_async_remote_copy(
        src_ref=src, dst_ref=dst, send_sem=send, recv_sem=recv, device_id=device, device_id_type=MESH
    )


def greet(devices):
    barrier = pltpu.get_barrier_semaphore()
    for device in devices:
        pl.semaphore_signal(barrier, inc=1, device_id=device, device_id_type=MESH)
    pl.semaphore_wait(barrier, len(devices))


class Place:
    def __init__(self, sp, tp):
        self.sp, self.tp, self.Z, self.Y = sp, tp, sp // 2, tp // 2
        self.s, self.t = lax.axis_index("sp"), lax.axis_index("tp")
        self.z, self.x = self.s // 2, self.s % 2
        self.y, self.c = self.t // 2, self.t % 2
        self.partner = (self.s, self.y * 2 + 1 - self.c)
        self.across = (self.z * 2 + 1 - self.x, self.t)

    def chip_y(self, d):
        return (self.s, lax.rem(self.y + d + self.Y, self.Y) * 2 + self.c)

    def chip_z(self, d):
        return (lax.rem(self.z + d + self.Z, self.Z) * 2 + self.x, self.t)


class LineGather:
    def __init__(self, place, pairs, up_s, up_r, dn_s, dn_r, x_s, x_r):
        self.p, self.pairs = place, pairs
        self.sems = (up_s, up_r, dn_s, dn_r, x_s, x_r)

    def up(self, n, d, own=False):
        p, (own_ref, all_ref) = self.p, self.pairs[n]
        block = p.s - 2 * (d - 1)
        src = own_ref if own else all_ref.at[block]
        return push(src, all_ref.at[block], self.sems[0].at[n, d], self.sems[1].at[n, d], (p.s + 2, p.t))

    def up_wait(self, n, d):
        p, (_, all_ref) = self.p, self.pairs[n]
        ref = all_ref.at[p.s - 2 * d]
        return push(ref, ref, self.sems[0].at[n, d], self.sems[1].at[n, d], (p.s - 2, p.t))

    def dn(self, n, d, own=False):
        p, (own_ref, all_ref) = self.p, self.pairs[n]
        block = p.s + 2 * (d - 1)
        src = own_ref if own else all_ref.at[block]
        return push(src, all_ref.at[block], self.sems[2].at[n, d], self.sems[3].at[n, d], (p.s - 2, p.t))

    def dn_wait(self, n, d):
        p, (_, all_ref) = self.p, self.pairs[n]
        ref = all_ref.at[p.s + 2 * d]
        return push(ref, ref, self.sems[2].at[n, d], self.sems[3].at[n, d], (p.s + 2, p.t))

    def over(self, n, d):
        p, (own_ref, all_ref) = self.p, self.pairs[n]
        block = p.s - 2 * d
        k = d + p.Z - 1
        src = own_ref if d == 0 else all_ref.at[block]
        return push(src, all_ref.at[block], self.sems[4].at[n, k], self.sems[5].at[n, k], p.across)

    def over_wait(self, n, d):
        p, (_, all_ref) = self.p, self.pairs[n]
        ref = all_ref.at[p.z * 2 + 1 - p.x - 2 * d]
        k = d + p.Z - 1
        return push(ref, ref, self.sems[4].at[n, k], self.sems[5].at[n, k], p.across)

    def start(self, count):
        p = self.p

        @pl.when(p.z + 1 < p.Z)
        def _():
            for n in count:
                self.up(n, 1, True).start()

        @pl.when(p.z >= 1)
        def _():
            for n in count:
                self.dn(n, 1, True).start()

        for n in count:
            self.over(n, 0).start()

    def step(self, d):
        p = self.p
        for n in range(len(self.pairs)):

            @pl.when(p.z - d >= 0)
            def _():
                self.up_wait(n, d).wait_recv()

                @pl.when(p.z + 1 < p.Z)
                def _():
                    self.up(n, d + 1).start()

                self.over(n, d).start()

            @pl.when(p.z + d < p.Z)
            def _():
                self.dn_wait(n, d).wait_recv()

                @pl.when(p.z >= 1)
                def _():
                    self.dn(n, d + 1).start()

                self.over(n, -d).start()

    def arrive(self, sign, d):
        for n in range(len(self.pairs)):
            self.over_wait(n, sign * d).wait_recv()

    def side(self, sign, d):
        return self.p.z - d >= 0 if sign > 0 else self.p.z + d < self.p.Z

    def finish(self):
        p = self.p
        for n in range(len(self.pairs)):
            for d in range(p.Z):
                for sign in (1, -1) if d else (1,):

                    @pl.when(self.side(sign, d))
                    def _():
                        self.over(n, sign * d).wait_send()

            for d in range(1, p.Z):

                @pl.when(jnp.logical_and(p.z - d + 1 >= 0, p.z + 1 < p.Z))
                def _():
                    self.up(n, d).wait_send()

                @pl.when(jnp.logical_and(p.z + d - 1 < p.Z, p.z >= 1))
                def _():
                    self.dn(n, d).wait_send()


def line_sems(p_z, n):
    return [pltpu.SemaphoreType.DMA((n, p_z + 1))] * 4 + [pltpu.SemaphoreType.DMA((n, 2 * p_z))] * 2


class PairScatter:
    def __init__(self, p, part, first, summed, second, fs, fr, ss, sr):
        self.p, self.part, self.first, self.summed, self.second = p, part, first, summed, second
        self.sems = (fs, fr, ss, sr)
        self.started = []

    def start(self):
        p = self.p
        for d in range(p.Y):
            y = lax.rem(p.y + d, p.Y)
            copy = push(
                self.part(y * 2 + 1 - p.c), self.first.at[d], self.sems[0].at[d], self.sems[1].at[d], p.partner
            )
            copy.start()
            self.started.append(copy)

    def middle(self):
        p = self.p
        for d in list(range(1, p.Y)) + [0]:
            y = lax.rem(p.y + d, p.Y)
            self.started[d].wait_recv()
            total = self.part(y * 2 + p.c)[...].astype(F32) + self.first[d].astype(F32)
            self.summed[d] = total.astype(BF)
            if d:
                copy = push(
                    self.summed.at[d], self.second.at[d], self.sems[2].at[d], self.sems[3].at[d], p.chip_y(d)
                )
                copy.start()
                self.started.append(copy)

    def finish(self):
        p = self.p
        total = self.part(p.t)[...].astype(F32) + self.first[0].astype(F32)
        for d in range(1, p.Y):
            self.started[p.Y + d - 1].wait_recv()
            total = total + self.second[d].astype(F32)
        for copy in self.started:
            copy.wait_send()
        return total


class PairGather:
    def __init__(self, p, own, spot, ys, yr, ps, pr):
        self.p, self.own, self.spot, self.sems = p, own, spot, (ys, yr, ps, pr)
        self.started = []

    def start(self):
        p = self.p
        for d in range(1, p.Y):
            copy = push(self.own, self.spot(p.t), self.sems[0].at[d], self.sems[1].at[d], p.chip_y(d))
            copy.start()
            self.started.append(copy)
        copy = push(self.own, self.spot(p.t), self.sems[2].at[0], self.sems[3].at[0], p.partner)
        copy.start()
        self.started.append(copy)

    def forward(self):
        p = self.p
        for d in range(1, p.Y):
            ref = self.spot(lax.rem(p.y - d + p.Y, p.Y) * 2 + p.c)
            push(ref, ref, self.sems[0].at[d], self.sems[1].at[d], p.chip_y(-d)).wait_recv()
            copy = push(ref, ref, self.sems[2].at[d], self.sems[3].at[d], p.partner)
            copy.start()
            self.started.append(copy)

    def arrive(self):
        p = self.p
        for d in range(p.Y):
            ref = self.spot(lax.rem(p.y - d + p.Y, p.Y) * 2 + 1 - p.c)
            push(ref, ref, self.sems[2].at[d], self.sems[3].at[d], p.partner).wait_recv()

    def finish(self):
        for copy in self.started:
            copy.wait_send()


def layer_kernel(
    sp, tp, shift_base,
    raw, to, src, gain, saved, offs, wq_h, wk_h, wv_h, wo_h,
    flat_all, src_out, tgt_out, cols_all,
    tn, pieces, wq, wk, wv, wo, tn_all, to_all, src_all, cols, tn_b, to_b,
    q_all, hg_all, small_all, k_s, v_s, p_s, d_s, part, kf, vf, sg,
    xr, xz, zr, sg1, sg2, sg3, ng, ng1, ng2, ng3,
    wsem, loc, es, er, *sems
):
    p = Place(sp, tp)
    pair_sems = [sems[4 * i : 4 * i + 4] for i in range(6)]
    xs_s, xs_r, zs_s, zs_r = sems[24:28]
    line_a, line_b = sems[28:34], sems[34:40]
    rows, block = raw.shape[0], saved.shape[0]
    width, model = wq.shape[1], wq.shape[0]
    heads = width // HEAD_DIM
    scale = HEAD_DIM ** (-0.5)
    loads = [
        pltpu.make_async_copy(h, v, wsem.at[i])
        for i, (h, v) in enumerate(((wq_h, wq), (wo_h, wo), (wk_h, wk), (wv_h, wv)))
    ]
    for copy in loads:
        copy.start()
    raw_value, gain_value = raw[...].astype(F32), gain[...].astype(F32).reshape(1, model)
    inverse = lax.rsqrt(jnp.mean(raw_value * raw_value, axis=1, keepdims=True) + EPSILON)
    normed_value = (raw_value * inverse * gain_value).astype(BF)
    tn[...] = normed_value
    slice_width = model // sp
    for s in range(sp):
        pieces[s] = normed_value[:, s * slice_width : (s + 1) * slice_width]
    greet(
        [p.partner]
        + [p.chip_y(d) for d in range(1, p.Y)]
        + [(lax.rem(p.s + e, sp), p.t) for e in range(1, sp)]
    )
    g_tn = PairGather(p, tn, lambda t: tn_all.at[t], *pair_sems[0])
    g_to = PairGather(p, to, lambda t: to_all.at[t], *pair_sems[1])
    g_src = PairGather(p, src, lambda t: src_all.at[t], *pair_sems[2])
    g_cols = PairGather(p, cols, lambda t: cols_all.at[:, t], *pair_sems[3])
    for g in (g_tn, g_to, g_src):
        g.start()
    swaps = []
    for e in range(1, sp):
        s = lax.rem(p.s + e, sp)
        copy = push(pieces.at[s], cols.at[p.s], es.at[e], er.at[e], (s, p.t))
        copy.start()
        swaps.append(copy)
    mine = [
        pltpu.make_async_copy(tn, tn_all.at[p.t], loc.at[0]),
        pltpu.make_async_copy(to, to_all.at[p.t], loc.at[1]),
        pltpu.make_async_copy(src, src_all.at[p.t], loc.at[2]),
        pltpu.make_async_copy(pieces.at[p.s], cols.at[p.s], loc.at[3]),
    ]
    for copy in mine:
        copy.start()
    for copy in mine:
        copy.wait()
    tile = min(width, 256)
    gather = LineGather(
        p, ((q_all.at[p.s], q_all), (hg_all.at[p.s], hg_all), (small_all.at[p.s], small_all)), *line_a
    )

    g_tn.forward()
    g_to.forward()
    g_tn.arrive()
    for t in range(tp):
        tn_b[t * rows : (t + 1) * rows, :] = tn_all[t]
    loads[0].wait()
    for j in range(0, width, tile):
        q_all[p.s, :, j : j + tile] = jnp.dot(
            tn_b[...], wq[:, j : j + tile], preferred_element_type=F32
        ).astype(BF)
    gather.start((0,))
    g_to.arrive()
    for t in range(tp):
        to_b[t * rows : (t + 1) * rows, :] = to_all[t]
    loads[1].wait()
    lane = lax.broadcasted_iota(jnp.int32, (block, 128), 1)
    pick = lax.broadcasted_iota(jnp.int32, (heads, 128), 0) == lax.broadcasted_iota(jnp.int32, (heads, 128), 1)
    small = lax.dot_general(
        offs[...].astype(F32), pick.astype(F32), (((0,), (0,)), ((), ())), precision=lax.Precision.HIGHEST,
        preferred_element_type=F32,
    )
    for h in range(heads):
        cut = slice(h * HEAD_DIM, (h + 1) * HEAD_DIM)
        part_h = contract_last(to_b[...], wo[cut, :]).astype(BF)
        hg_all[p.s, :, cut] = part_h
        delta = jnp.sum(part_h.astype(F32) * saved[:, cut].astype(F32), axis=1, keepdims=True)
        small = jnp.where(lane == heads + h, delta, small)
    small_all[p.s] = small.astype(BF)
    gather.start((1, 2))

    g_src.forward()
    g_src.arrive()
    gather.step(1)
    source_count = k_s.shape[0]
    loads[2].wait()
    loads[3].wait()

    @pl.loop(0, width // tile)
    def _(j):
        cut = pl.ds(pl.multiple_of(j * tile, tile), tile)
        rows_value = src_all[...].reshape(source_count, model)
        k_s[:, cut] = jnp.dot(rows_value, wk[:, cut], preferred_element_type=F32).astype(BF)
        v_s[:, cut] = jnp.dot(rows_value, wv[:, cut], preferred_element_type=F32).astype(BF)

    for e in range(1, sp):
        s = lax.rem(p.s - e + sp, sp)
        push(cols.at[s], cols.at[s], es.at[e], er.at[e], (s, p.t)).wait_recv()
    g_cols.start()
    keep = pltpu.make_async_copy(cols, cols_all.at[:, p.t], loc.at[4])
    keep.start()

    def into(k):
        z = lax.rem(p.z + k, p.Z)
        return push(part.at[z * 2 + 1 - p.x], xr.at[k], xs_s.at[k], xs_r.at[k], p.across)

    def attend(z):
        pair = pl.ds(2 * z, 2)
        spot = pl.ds(pl.multiple_of(z * (2 * block), 2 * block), 2 * block)
        tiny = small_all[pair].reshape(2 * block, 128).astype(F32)
        for h in range(heads):
            cut = slice(h * HEAD_DIM, (h + 1) * HEAD_DIM)
            q_h = q_all[pair, :, cut].reshape(2 * block, HEAD_DIM)
            g_h = hg_all[pair, :, cut].reshape(2 * block, HEAD_DIM)
            prob = jnp.exp(contract_last(q_h, k_s[:, cut]) * scale - (shift_base + tiny[:, h : h + 1]))
            grad = contract_last(g_h, v_s[:, cut])
            score = (prob * (grad - tiny[:, heads + h : heads + h + 1]) * scale).astype(BF)
            p_s[h, spot, :] = prob.astype(BF)
            d_s[h, spot, :] = score
            term = jnp.dot(score, k_s[:, cut], preferred_element_type=F32).astype(BF)
            part[pair, :, cut] = term.reshape(2, block, HEAD_DIM)

    def reached(sign, d):
        gather.arrive(sign, d)
        attend(p.z - sign * d)
        into((-sign * d) % p.Z).start()

    for d in range(1, p.Z):
        if d > 1:
            gather.step(d)
        for sign in (1, -1) if d > 1 else (1,):

            @pl.when(gather.side(sign, d - 1))
            def _():
                reached(sign, d - 1)

        if d == 1:
            g_cols.forward()
    for sign in (1, -1):

        @pl.when(gather.side(sign, p.Z - 1))
        def _():
            reached(sign, p.Z - 1)

    order = sorted(range(1, p.Z), key=lambda k: min(k, p.Z - k))
    hops = {}

    def relay(k):
        into(k).wait_recv()
        z = lax.rem(p.z + k, p.Z)
        xz[k] = (part[z * 2 + p.x].astype(F32) + xr[k].astype(F32)).astype(BF)
        hops[k] = push(xz.at[k], zr.at[k], zs_s.at[k], zs_r.at[k], p.chip_z(k))
        hops[k].start()

    for k in order[:1]:
        relay(k)
    count = sp * block

    for h in range(heads):
        cut = slice(h * HEAD_DIM, (h + 1) * HEAD_DIM)
        dims = (((0,), (0,)), ((), ()))
        q_h = q_all[:, :, cut].reshape(count, HEAD_DIM)
        g_h = hg_all[:, :, cut].reshape(count, HEAD_DIM)
        kf[:, cut] = lax.dot_general(d_s[h], q_h, dims, preferred_element_type=F32).astype(BF)
        vf[:, cut] = lax.dot_general(p_s[h], g_h, dims, preferred_element_type=F32).astype(BF)
    for k in order[1:2]:
        relay(k)
    stile = min(model, 256)

    def source_term(j):
        cut = pl.ds(pl.multiple_of(j * stile, stile), stile)
        value = contract_last(kf[...], wk[cut, :]) + contract_last(vf[...], wv[cut, :])
        sg[:, :, cut] = value.astype(BF).reshape(tp, source_count // tp, stile)

    half = model // stile // 2
    pl.loop(0, half)(source_term)
    for k in order[2:]:
        relay(k)
    pl.loop(half, model // stile)(source_term)
    source = PairScatter(p, lambda t: sg.at[t], sg1, sg2, sg3, *pair_sems[4])
    source.start()
    source.middle()
    into(0).wait_recv()
    total = part[p.s].astype(F32) + xr[0].astype(F32)
    for k in order:
        hops[k].wait_recv()
        total = total + zr[k].astype(F32)
    flat = total.astype(BF)
    flat_all[p.s] = flat
    spread = LineGather(p, ((flat_all.at[p.s], flat_all),), *line_b)
    spread.start((0,))
    for j in range(0, model, stile):
        columns = contract_last(flat, wq[j : j + stile, :]).astype(BF)
        for t in range(tp):
            ng[t, :, j : j + stile] = columns[t * rows : (t + 1) * rows]
    normed = PairScatter(p, lambda t: ng.at[t], ng1, ng2, ng3, *pair_sems[5])
    normed.start()
    for d in range(1, p.Z):
        spread.step(d)
        if d == 1:
            normed.middle()
    src_out[...] = source.finish()
    raw_value, gain_value = raw[...].astype(F32), gain[...].astype(F32).reshape(1, model)
    inverse = lax.rsqrt(jnp.mean(raw_value * raw_value, axis=1, keepdims=True) + EPSILON)
    scaled = normed.finish() * gain_value
    tgt_out[...] = inverse * scaled - raw_value * (inverse * inverse * inverse) * jnp.mean(
        scaled * raw_value, axis=1, keepdims=True
    )
    g_cols.arrive()
    for d in range(p.Z):
        for sign in (1, -1) if d else (1,):

            @pl.when(spread.side(sign, d))
            def _():
                spread.arrive(sign, d)

    gather.finish()
    spread.finish()
    for g in (g_tn, g_to, g_src, g_cols):
        g.finish()
    for copy in swaps:
        copy.wait_send()
    keep.wait()
    for k in range(p.Z):
        into(k).wait_send()
    for k in order:
        hops[k].wait_send()


def body(
    target_rows,
    source_rows,
    norm_gain,
    query_weight,
    key_weight,
    value_weight,
    output_weight,
    saved_output,
    norm_offset,
    output_grad,
):
    tp, sp = lax.axis_size("tp"), lax.axis_size("sp")
    Z, Y = sp // 2, tp // 2
    model, width = query_weight.shape
    heads = width // HEAD_DIM
    rows, srows = target_rows.shape[0], source_rows.shape[0]
    block = rows * tp
    count = block * sp
    source_count = srows * tp
    shift_base = math.log(source_count * sp)
    slice_width = model // sp
    dma = pltpu.SemaphoreType.DMA

    vm = pltpu.VMEM
    whole = pl.BlockSpec(memory_space=pl.ANY)
    flat_all, source_grad, target_grad, cols_all = pl.pallas_call(
        functools.partial(layer_kernel, sp, tp, shift_base),
        out_shape=[
            jax.ShapeDtypeStruct((sp, block, width), BF),
            jax.ShapeDtypeStruct((srows, model), F32),
            jax.ShapeDtypeStruct((rows, model), F32),
            jax.ShapeDtypeStruct((sp, tp, rows, slice_width), BF),
        ],
        in_specs=[VMEM] * 6 + [whole] * 4,
        out_specs=[VMEM] * 4,
        scratch_shapes=[vm((rows, model), BF), vm((sp, rows, slice_width), BF)]
        + [vm((model, width), BF)] * 3
        + [vm((width, model), BF)]
        + [vm((tp, rows, model), BF)] * 2
        + [vm((tp, srows, model), BF), vm((sp, rows, slice_width), BF)]
        + [vm((block, model), BF)] * 2
        + [vm((sp, block, width), BF)] * 2
        + [vm((sp, block, 128), BF)]
        + [vm((source_count, width), BF)] * 2
        + [vm((heads, count, source_count), BF)] * 2
        + [vm((sp, block, width), BF)]
        + [vm((source_count, width), BF)] * 2
        + [vm((tp, srows, model), BF)]
        + [vm((Z, block, width), BF)] * 3
        + [vm((Y, srows, model), BF)] * 3
        + [vm((tp, rows, model), BF)]
        + [vm((Y, rows, model), BF)] * 3
        + [dma((4,)), dma((5,)), dma((sp,)), dma((sp,))]
        + [dma((Y,))] * 24
        + [dma((Z,))] * 4
        + line_sems(Z, 3)
        + line_sems(Z, 1),
        name="layer_kernel",
        compiler_params=pltpu.CompilerParams(
            collective_id=1, has_side_effects=True, vmem_limit_bytes=58 * 2**20
        ),
    )(
        target_rows,
        output_grad,
        source_rows,
        norm_gain,
        saved_output,
        norm_offset.T,
        query_weight,
        key_weight,
        value_weight,
        output_weight,
    )
    weight_grad = lax.dot_general(
        cols_all.reshape(count, slice_width),
        flat_all.reshape(count, width),
        (((0,), (0,)), ((), ())),
        preferred_element_type=F32,
    )
    return (target_grad, source_grad, weight_grad)


def solution(mesh):
    in_specs = (
        P(("sp", "tp"), None),
        P(("sp", "tp"), None),
        P(),
        P(None, "tp"),
        P(None, "tp"),
        P(None, "tp"),
        P("tp", None),
        P("sp", "tp"),
        P("sp", "tp"),
        P(("sp", "tp"), None),
    )
    out_specs = (P(("sp", "tp"), None), P(("sp", "tp"), None), P("sp", "tp"))
    return jax.shard_map(body, mesh=mesh, in_specs=in_specs, out_specs=out_specs, check_vma=False)
```

profile of v0, /device:TPU:0, one launch (start us, length us, event | category | flops | bytes accessed | tf_op | source)
XLA Modules:
  0.0 87.9 jit_solution(5381410254483352762)
XLA Ops:
  0.6 81.0 %layer_kernel.1 = (bf16[8,64,1024]{2,1,0:T(8,128)(2,1)}, f32[64,2048]{1,0:T(8,128)}, f32[16,2048]{1,0:T(8,128)}, bf16[8,4,16,256]{3,2,1,0:T(8,128)(2,1)}) custom-call(bf16[16,2048]{1,0:T(8,128)(2,1)} %raw.1, bf16[16,2048]{1,0:T(8,128)(2,1)} %to.1, bf16[64,2048]{1,0:T(8,128)(2,1)} %src.1, bf16[2048]{0:T(1024)(128)(2,1)} %gain.1, bf16[64,1024]{1,0:T(8,128)(2,1)} %saved.1, ...), custom_call_target="tpu_custom_call" | custom-call | tf_op jit(solution)/shard_map/layer_kernel/pallas_call | solution.py:506
  81.7 2.8 %fusion = f32[256,1024]{1,0:T(8,128)} fusion(bf16[512,256]{1,0:T(8,128)(2,1)} %bitcast.6, bf16[512,1024]{1,0:T(8,128)(2,1)} %bitcast.5), kind=kOutput, calls=%fused_computation | convolution fusion | flops 268435456 | bytes 2359296 | tf_op jit(solution)/shard_map/dot_general | solution.py:554
  84.4 1.6 %copy.15 = f32[16,2048]{1,0:T(8,128)} copy(f32[16,2048]{1,0:T(8,128)} %get-tuple-element.14) | data formatting | bytes 262144
  86.0 1.9 %copy.16 = f32[64,2048]{1,0:T(8,128)} copy(f32[64,2048]{1,0:T(8,128)} %get-tuple-element.15) | data formatting | bytes 1048576
where the time goes:
time: 88.1 us; the launch traced here: 87.9 us
  Pallas kernels  81 us (92%)
  local copies, waits for them, and re-layouts  3.44 us (4%)
  matrix products  2.76 us (3%)
    pallas_call x1, Pallas kernels, body(): pl.pallas_call(functools.partial(layer_kernel, sp, tp, shift_base), out_s...  81 us
    unnamed x2, local copies, waits for them, and re-layouts  3.44 us
    dot_general x1, matrix products, body(): lax.dot_general(cols_all.reshape(count, slice_width), flat_all.reshape(co...  2.76 us

commit v1 on v0

--- a/solution.py
+++ b/solution.py
@@ -560,6 +560,443 @@
     return (target_grad, source_grad, weight_grad)
 
 
+class Net:
+    def __init__(self, send, recv):
+        self.sems, self.ids, self.started = (send, recv), {}, []
+
+    def _copy(self, name, src, dst, device):
+        n = self.ids.setdefault(name, len(self.ids))
+        return push(src, dst, self.sems[0].at[n], self.sems[1].at[n], device)
+
+    def go(self, name, src, dst, device):
+        copy = self._copy(name, src, dst, device)
+        copy.start()
+        self.started.append(copy)
+
+    def wait(self, name, landed, device):
+        self._copy(name, landed, landed, device).wait_recv()
+
+    def close(self):
+        for copy in self.started:
+            copy.wait_send()
+
+
+TRANSFERS = 160
+
+
+def grid_kernel(
+    sp, tp, shift_base,
+    raw, to, src, gain, saved, offs, wq_h, wk_h, wv_h, wo_h,
+    ws, src_out, tgt_out,
+    tn_all, to_all, src_all, pieces, cols, q_st, g_st, sm_st, q_all, g_all, sm_all,
+    wq, wk, wv, wo, k_s, v_s, p_s, d_s, part, xr, xz, zr, flat_all, fl, kf, vf,
+    sg, sd, ss, es, fs, fr, ng, ng1, ng2, ng3, wt,
+    wsem, send, recv, *sems
+):
+    p = Place(sp, tp)
+    s, t, y, c, x = p.s, p.t, p.y, p.c, p.x
+    u, v = p.z // 2, p.z % 2
+    net = Net(send, recv)
+
+    def at(u, v, x):
+        return ((u * 2 + v) * 2 + x, t)
+
+    C, Y, V, X, U = p.partner, p.chip_y(1), at(u, 1 - v, x), at(u, v, 1 - x), at(1 - u, v, x)
+    ty, tc, tyc = (1 - y) * 2 + c, y * 2 + 1 - c, (1 - y) * 2 + 1 - c
+    rows, block, srows = raw.shape[0], saved.shape[0], src.shape[0]
+    model, width = wq.shape
+    heads = width // HEAD_DIM
+    hh, half = heads // 2, width // 2
+    sblock = srows * tp
+    sw = model // sp
+    scale = HEAD_DIM ** (-0.5)
+    mine = pl.ds(pl.multiple_of(v * half, half), half)
+    loads = [
+        pltpu.make_async_copy(h, w, wsem.at[i])
+        for i, (h, w) in enumerate(((wq_h, wq), (wo_h, wo), (wk_h.at[:, mine], wk), (wv_h.at[:, mine], wv)))
+    ]
+    for copy in loads:
+        copy.start()
+    raw_value, gain_value = raw[...].astype(F32), gain[...].astype(F32).reshape(1, model)
+    inverse = lax.rsqrt(jnp.mean(raw_value * raw_value, axis=1, keepdims=True) + EPSILON)
+    normed_value = (raw_value * inverse * gain_value).astype(BF)
+    tn_all[t] = normed_value
+    to_all[t] = to[...]
+    src_all[v, t] = src[...]
+    for a in range(2):
+        for b in range(2):
+            for k in range(2):
+                n = (2 * a + k) * 2 + b
+                pieces[a, b, :, k * sw : (k + 1) * sw] = normed_value[:, n * sw : (n + 1) * sw]
+    others = [
+        (a, b, d, u + a - 2 * u * a, v + b - 2 * v * b, x + d - 2 * x * d)
+        for a in range(2) for b in range(2) for d in range(2) if a + b + d
+    ]
+    greet([C, Y] + [at(*o[3:]) for o in others])
+    A, B = pl.ds(0, srows // 2), pl.ds(srows // 2, srows // 2)
+
+    def same(name, ref, device):
+        net.go(name, ref, ref, device)
+
+    same("tnY", tn_all.at[t], Y)
+    same("sVB", src_all.at[v, t, B], V)
+    same("tnC", tn_all.at[t], C)
+    same("toY", to_all.at[t], Y)
+    same("toC", to_all.at[t], C)
+    same("sYA", src_all.at[v, t, A], Y)
+    same("sVA", src_all.at[v, t, A], V)
+    same("sYB", src_all.at[v, t, B], Y)
+    same("sC", src_all.at[v, t], C)
+    spot = (u * 2 + x) * 2 + v
+    for a, b, d, u2, v2, x2 in others:
+        net.go(f"p{a}{b}{d}", pieces.at[u2, x2], cols.at[spot, t], at(u2, v2, x2))
+    cols[spot, t] = pieces[u, x]
+
+    net.wait("tnY", tn_all.at[ty], Y)
+    same("tnF", tn_all.at[ty], C)
+    net.wait("toY", to_all.at[ty], Y)
+    same("toF", to_all.at[ty], C)
+    net.wait("tnC", tn_all.at[tc], C)
+    net.wait("tnF", tn_all.at[tyc], C)
+    loads[0].wait()
+    tn_b = tn_all[...].reshape(block, model)
+    for k in range(2):
+        for j in range(0, half, HEAD_DIM):
+            q_st[k, :, j : j + HEAD_DIM] = jnp.dot(
+                tn_b, wq[:, k * half + j : k * half + j + HEAD_DIM], preferred_element_type=F32
+            ).astype(BF)
+    net.go("qV", q_st.at[1 - v], q_all.at[u, x, v], V)
+    q_all[u, x, v] = q_st[v]
+    same("q0U", q_all.at[u, x, v], U)
+    same("q0X", q_all.at[u, x, v], X)
+    net.wait("toC", to_all.at[tc], C)
+    net.wait("toF", to_all.at[tyc], C)
+    loads[1].wait()
+    to_b = to_all[...].reshape(block, model)
+    lines, lanes = sm_st.shape[1], 2 * block
+    line = lax.broadcasted_iota(jnp.int32, (lines, lanes), 0)
+    place = (
+        lax.broadcasted_iota(jnp.int32, (block, lanes), 1)
+        == lax.broadcasted_iota(jnp.int32, (block, lanes), 0) + v * block
+    ).astype(F32)
+    spread = jnp.dot(offs[...].astype(F32), place, precision=lax.Precision.HIGHEST, preferred_element_type=F32)
+    ones = jnp.ones((lines, HEAD_DIM), F32)
+    for k in range(2):
+        small = jnp.zeros((lines, lanes), F32)
+        for h in range(hh):
+            n = k * hh + h
+            cut = slice(n * HEAD_DIM, (n + 1) * HEAD_DIM)
+            part_h = contract_last(to_b, wo[cut, :]).astype(BF)
+            g_st[k, :, h * HEAD_DIM : (h + 1) * HEAD_DIM] = part_h
+            product = part_h.astype(F32) * saved[:, cut].astype(F32)
+            padded = jnp.concatenate(
+                [jnp.where(v == 0, product, 0.0), jnp.where(v == 1, product, 0.0)], axis=0
+            )
+            delta = lax.dot_general(
+                ones, padded, (((1,), (1,)), ((), ())), precision=lax.Precision.HIGHEST, preferred_element_type=F32
+            )
+            small = jnp.where(line == h, jnp.broadcast_to(spread[n : n + 1], small.shape), small)
+            small = jnp.where(line == hh + h, delta, small)
+        sm_st[k] = small.astype(BF)
+    net.go("mV", sm_st.at[1 - v], sm_all.at[u, x, v], V)
+    net.go("gV", g_st.at[1 - v], g_all.at[u, x, v], V)
+    g_all[u, x, v] = g_st[v]
+    sm_all[u, x, v] = sm_st[v]
+    same("m0U", sm_all.at[u, x, v], U)
+    same("g0U", g_all.at[u, x, v], U)
+    same("m0X", sm_all.at[u, x, v], X)
+    same("g0X", g_all.at[u, x, v], X)
+
+    net.wait("sVB", src_all.at[1 - v, t, B], V)
+    same("fVB", src_all.at[1 - v, t, B], Y)
+    same("cVB", src_all.at[1 - v, t, B], C)
+    net.wait("sYA", src_all.at[v, ty, A], Y)
+    same("fYA", src_all.at[v, ty, A], V)
+    same("cYA", src_all.at[v, ty, A], C)
+    net.wait("qV", q_all.at[u, x, 1 - v], V)
+    same("q1U", q_all.at[u, x, 1 - v], U)
+    same("q1X", q_all.at[u, x, 1 - v], X)
+    net.wait("sVA", src_all.at[1 - v, t, A], V)
+    same("cVA", src_all.at[1 - v, t, A], C)
+    net.wait("sYB", src_all.at[v, ty, B], Y)
+    same("cYB", src_all.at[v, ty, B], C)
+    net.wait("mV", sm_all.at[u, x, 1 - v], V)
+    net.wait("gV", g_all.at[u, x, 1 - v], V)
+    same("m1U", sm_all.at[u, x, 1 - v], U)
+    same("g1U", g_all.at[u, x, 1 - v], U)
+    same("m1X", sm_all.at[u, x, 1 - v], X)
+    same("g1X", g_all.at[u, x, 1 - v], X)
+    for a, b, d, u2, v2, x2 in others:
+        net.wait(f"p{a}{b}{d}", cols.at[(u2 * 2 + x2) * 2 + v2, t], at(u2, v2, x2))
+    same("kY", cols.at[:, t], Y)
+    same("kC", cols.at[:, t], C)
+    net.wait("q0U", q_all.at[1 - u, x, v], U)
+    same("q2X", q_all.at[1 - u, x, v], X)
+    net.wait("fVB", src_all.at[1 - v, ty, B], Y)
+    same("dVB", src_all.at[1 - v, ty, B], C)
+    net.wait("fYA", src_all.at[1 - v, ty, A], V)
+    same("dYA", src_all.at[1 - v, ty, A], C)
+
+    def project(k):
+        spot = pl.ds(pl.multiple_of(k * sblock, sblock), sblock)
+
+        @pl.loop(0, half // HEAD_DIM)
+        def _(j):
+            cut = pl.ds(pl.multiple_of(j * HEAD_DIM, HEAD_DIM), HEAD_DIM)
+            value = src_all[k].reshape(sblock, model)
+            k_s[spot, cut] = jnp.dot(value, wk[:, cut], preferred_element_type=F32).astype(BF)
+            v_s[spot, cut] = jnp.dot(value, wv[:, cut], preferred_element_type=F32).astype(BF)
+
+    net.wait("sC", src_all.at[v, tc], C)
+    net.wait("cYA", src_all.at[v, tyc, A], C)
+    net.wait("cYB", src_all.at[v, tyc, B], C)
+    loads[2].wait()
+    loads[3].wait()
+    project(v)
+    net.wait("q1U", q_all.at[1 - u, x, 1 - v], U)
+    same("q3X", q_all.at[1 - u, x, 1 - v], X)
+    net.wait("cVB", src_all.at[1 - v, tc, B], C)
+    net.wait("cVA", src_all.at[1 - v, tc, A], C)
+    net.wait("dVB", src_all.at[1 - v, tyc, B], C)
+    net.wait("dYA", src_all.at[1 - v, tyc, A], C)
+    project(1 - v)
+    net.wait("m0U", sm_all.at[1 - u, x, v], U)
+    same("m2X", sm_all.at[1 - u, x, v], X)
+    net.wait("g0U", g_all.at[1 - u, x, v], U)
+    same("g2X", g_all.at[1 - u, x, v], X)
+
+    def attend(w, after=None):
+        little = sm_all[w].astype(F32)
+        little = jnp.concatenate([little[0, 0] + little[0, 1], little[1, 0] + little[1, 1]], axis=1)
+        for h in range(hh):
+            cut = slice(h * HEAD_DIM, (h + 1) * HEAD_DIM)
+            q_h = q_all[w, :, :, :, cut].reshape(4 * block, HEAD_DIM)
+            g_h = g_all[w, :, :, :, cut].reshape(4 * block, HEAD_DIM)
+            prob = jnp.exp(contract_last(k_s[:, cut], q_h) * scale - (shift_base + little[h : h + 1]))
+            grad = contract_last(v_s[:, cut], g_h)
+            score = (prob * (grad - little[hh + h : hh + h + 1]) * scale).astype(BF)
+            p_s[w, h] = prob.astype(BF)
+            d_s[w, h] = score
+            term = lax.dot_general(score, k_s[:, cut], (((0,), (0,)), ((), ())), preferred_element_type=F32)
+            part[w, :, h] = term.astype(BF).reshape(2, 2, block, HEAD_DIM)
+            if after is not None:
+                after(h)
+
+    for n, k in ((0, v), (1, 1 - v)):
+        net.wait(f"q{n}X", q_all.at[u, 1 - x, k], X)
+        net.wait(f"m{n}X", sm_all.at[u, 1 - x, k], X)
+        net.wait(f"g{n}X", g_all.at[u, 1 - x, k], X)
+    attend(u)
+    net.go("aX", part.at[u, 1 - x], xr.at[0], X)
+    net.wait("m1U", sm_all.at[1 - u, x, 1 - v], U)
+    same("m3X", sm_all.at[1 - u, x, 1 - v], X)
+    net.wait("g1U", g_all.at[1 - u, x, 1 - v], U)
+    same("g3X", g_all.at[1 - u, x, 1 - v], X)
+    net.wait("kY", cols.at[:, ty], Y)
+    same("kF", cols.at[:, ty], C)
+    for n, k in ((2, v), (3, 1 - v)):
+        net.wait(f"q{n}X", q_all.at[1 - u, 1 - x, k], X)
+        net.wait(f"m{n}X", sm_all.at[1 - u, 1 - x, k], X)
+        net.wait(f"g{n}X", g_all.at[1 - u, 1 - x, k], X)
+    attend(1 - u, lambda h: net.go(f"b{h}X", part.at[1 - u, 1 - x, h], xr.at[1, h], X))
+    for h in range(hh):
+        cut = slice(h * HEAD_DIM, (h + 1) * HEAD_DIM)
+        k_h, v_h = 0.0, 0.0
+        for w in range(2):
+            q_h = q_all[w, :, :, :, cut].reshape(4 * block, HEAD_DIM)
+            g_h = g_all[w, :, :, :, cut].reshape(4 * block, HEAD_DIM)
+            k_h = k_h + jnp.dot(d_s[w, h], q_h, preferred_element_type=F32)
+            v_h = v_h + jnp.dot(p_s[w, h], g_h, preferred_element_type=F32)
+        kf[:, cut] = k_h.astype(BF)
+        vf[:, cut] = v_h.astype(BF)
+    stile = min(model // 2, 256)
+
+    def source_half(n):
+        @pl.loop(0, model // 2 // stile)
+        def _(j):
+            here = pl.ds(pl.multiple_of(n * (model // 2) + j * stile, stile), stile)
+            cut = pl.ds(pl.multiple_of(j * stile, stile), stile)
+            value = contract_last(kf[...], wk[here, :]) + contract_last(vf[...], wv[here, :])
+            sg[n, :, :, :, cut] = value.astype(BF).reshape(2, tp, srows, stile)
+
+        for a in range(2):
+            for b in range(2):
+                net.go(f"d{n}{a}{b}", sg.at[n, a, b * 2 + 1 - c], sd.at[n, a, b], C)
+
+    source_half(0)
+    source_half(1)
+    for h in range(hh):
+        net.wait(f"b{h}X", xr.at[1, h], X)
+        xz[h] = (part[1 - u, x, h].astype(F32) + xr[1, h].astype(F32)).astype(BF)
+        net.go(f"z{h}U", xz.at[h], zr.at[h], U)
+
+    def source_sum(n):
+        for a in range(2):
+            for b in range(2):
+                net.wait(f"d{n}{a}{b}", sd.at[n, a, b], C)
+                ss[n, a, b] = (sg[n, a, b * 2 + c].astype(F32) + sd[n, a, b].astype(F32)).astype(BF)
+
+    source_sum(0)
+    net.go("e01", ss.at[0, 1 - v, 1 - y], es.at[0, 1], Y)
+    net.go("e00", ss.at[0, v, 1 - y], es.at[0, 0], Y)
+    source_sum(1)
+    net.go("e11", ss.at[1, 1 - v, 1 - y], es.at[1, 1], V)
+    net.go("e10", ss.at[1, 1 - v, y], es.at[1, 0], V)
+    net.wait("aX", xr.at[0], X)
+    for h in range(hh):
+        net.wait(f"z{h}U", zr.at[h], U)
+        total = part[u, x, h].astype(F32) + xr[0, h].astype(F32) + zr[h].astype(F32)
+        flat_all[u, x, h] = total.astype(BF)
+        same(f"r{h}U", flat_all.at[u, x, h], U)
+        same(f"r{h}X", flat_all.at[u, x, h], X)
+        net.go(f"n{h}V", flat_all.at[u, x, h, 1 - v], fl.at[v, h], V)
+        fl[v, h] = flat_all[u, x, h, v]
+    net.wait("kC", cols.at[:, tc], C)
+    net.wait("kF", cols.at[:, tyc], C)
+    net.wait("e01", es.at[0, 1], Y)
+    fs[0] = (ss[0, 1 - v, y].astype(F32) + es[0, 1].astype(F32)).astype(BF)
+    net.go("f0", fs.at[0], fr.at[0], V)
+    net.wait("e11", es.at[1, 1], V)
+    fs[1] = (ss[1, v, 1 - y].astype(F32) + es[1, 1].astype(F32)).astype(BF)
+    net.go("f1", fs.at[1], fr.at[1], Y)
+    for h in range(hh):
+        net.wait(f"n{h}V", fl.at[1 - v, h], V)
+    ntile = min(model, 256)
+    for j in range(0, model, ntile):
+        columns = 0.0
+        for k in range(2):
+            for h in range(hh):
+                n = (k * hh + h) * HEAD_DIM
+                columns = columns + contract_last(fl[k, h], wq[j : j + ntile, n : n + HEAD_DIM])
+        ng[:, :, j : j + ntile] = columns.astype(BF).reshape(tp, rows, ntile)
+    normed = PairScatter(p, lambda n: ng.at[n], ng1, ng2, ng3, *sems)
+    normed.start()
+    net.wait("r0U", flat_all.at[1 - u, x, 0], U)
+    same("w0X", flat_all.at[1 - u, x, 0], X)
+    normed.middle()
+    for h in range(1, hh):
+        net.wait(f"r{h}U", flat_all.at[1 - u, x, h], U)
+        same(f"w{h}X", flat_all.at[1 - u, x, h], X)
+    cols_value = cols[...].reshape(sp * block, 2 * sw)
+    for h in range(hh):
+        net.wait(f"r{h}X", flat_all.at[u, 1 - x, h], X)
+        net.wait(f"w{h}X", flat_all.at[1 - u, 1 - x, h], X)
+        flat_h = flat_all[:, :, h].reshape(sp * block, HEAD_DIM)
+        for k in range(2):
+            wt[h, k] = lax.dot_general(
+                cols_value[:, k * sw : (k + 1) * sw], flat_h, (((0,), (0,)), ((), ())), preferred_element_type=F32
+            ).astype(BF)
+        net.go(f"W{h}", wt.at[h, 1 - v], ws.at[v, h], V)
+        ws[v, h] = wt[h, v]
+    for n, (key, last) in enumerate((("e00", Y), ("e10", V))):
+        net.wait(key, es.at[n, 0], last)
+        net.wait(f"f{n}", fr.at[n], (V, Y)[n])
+        src_out[:, n * (model // 2) : (n + 1) * (model // 2)] = (
+            ss[n, v, y].astype(F32) + es[n, 0].astype(F32) + fr[n].astype(F32)
+        )
+    raw_value, gain_value = raw[...].astype(F32), gain[...].astype(F32).reshape(1, model)
+    inverse = lax.rsqrt(jnp.mean(raw_value * raw_value, axis=1, keepdims=True) + EPSILON)
+    scaled = normed.finish() * gain_value
+    tgt_out[...] = inverse * scaled - raw_value * (inverse * inverse * inverse) * jnp.mean(
+        scaled * raw_value, axis=1, keepdims=True
+    )
+    for h in range(hh):
+        net.wait(f"W{h}", ws.at[1 - v, h], V)
+    net.close()
+
+
+def finish_kernel(ws, src_in, tgt_in, weight_out, src_out, tgt_out):
+    parts, hh = ws.shape[0], ws.shape[1]
+    for k in range(parts):
+        for h in range(hh):
+            n = (k * hh + h) * HEAD_DIM
+            weight_out[:, n : n + HEAD_DIM] = ws[k, h].astype(F32)
+    src_out[...] = src_in[...]
+    tgt_out[...] = tgt_in[...]
+
+
+def grid_body(
+    target_rows, source_rows, norm_gain, query_weight, key_weight, value_weight, output_weight,
+    saved_output, norm_offset, output_grad
+):
+    tp, sp = lax.axis_size("tp"), lax.axis_size("sp")
+    model, width = query_weight.shape
+    heads = width // HEAD_DIM
+    hh, half = heads // 2, width // 2
+    rows, srows = target_rows.shape[0], source_rows.shape[0]
+    block, sblock, sw = rows * tp, srows * tp, model // sp
+    Y = tp // 2
+    dma, vm = pltpu.SemaphoreType.DMA, pltpu.VMEM
+    whole = pl.BlockSpec(memory_space=pl.ANY)
+    pair = (2, 2, 2, block, half)
+    ws, source_grad, target_grad = pl.pallas_call(
+        functools.partial(grid_kernel, sp, tp, math.log(sblock * sp)),
+        out_shape=[
+            jax.ShapeDtypeStruct((2, hh, sw, HEAD_DIM), BF),
+            jax.ShapeDtypeStruct((srows, model), F32),
+            jax.ShapeDtypeStruct((rows, model), F32),
+        ],
+        in_specs=[VMEM] * 6 + [whole] * 4,
+        out_specs=[VMEM] * 3,
+        scratch_shapes=[vm((tp, rows, model), BF)] * 2
+        + [vm((2, tp, srows, model), BF)]
+        + [vm((2, 2, rows, 2 * sw), BF), vm((sp, tp, rows, 2 * sw), BF)]
+        + [vm((2, block, half), BF)] * 2
+        + [vm((2, 16, 2 * block), BF)]
+        + [vm(pair, BF)] * 2
+        + [vm((2, 2, 2, 16, 2 * block), BF)]
+        + [vm((model, width), BF)]
+        + [vm((model, half), BF)] * 2
+        + [vm((width, model), BF)]
+        + [vm((2 * sblock, half), BF)] * 2
+        + [vm((2, hh, 2 * sblock, 4 * block), BF)] * 2
+        + [vm((2, 2, hh, 2, block, HEAD_DIM), BF)]
+        + [vm((2, hh, 2, block, HEAD_DIM), BF)]
+        + [vm((hh, 2, block, HEAD_DIM), BF)] * 2
+        + [vm((2, 2, hh, 2, block, HEAD_DIM), BF)]
+        + [vm((2, hh, block, HEAD_DIM), BF)]
+        + [vm((2 * sblock, half), BF)] * 2
+        + [vm((2, 2, tp, srows, model // 2), BF)]
+        + [vm((2, 2, Y, srows, model // 2), BF)] * 2
+        + [vm((2, 2, srows, model // 2), BF)]
+        + [vm((2, srows, model // 2), BF)] * 2
+        + [vm((tp, rows, model), BF)]
+        + [vm((Y, rows, model), BF)] * 3
+        + [vm((hh, 2, sw, HEAD_DIM), BF)]
+        + [dma((4,)), dma((TRANSFERS,)), dma((TRANSFERS,))]
+        + [dma((Y,))] * 4,
+        name="grid_kernel",
+        compiler_params=pltpu.CompilerParams(
+            collective_id=1, has_side_effects=True, vmem_limit_bytes=58 * 2**20
+        ),
+    )(
+        target_rows, output_grad, source_rows, norm_gain, saved_output, norm_offset.T,
+        query_weight, key_weight, value_weight, output_weight,
+    )
+    weight_grad, source_grad, target_grad = pl.pallas_call(
+        finish_kernel,
+        out_shape=[
+            jax.ShapeDtypeStruct((sw, width), F32),
+            jax.ShapeDtypeStruct((srows, model), F32),
+            jax.ShapeDtypeStruct((rows, model), F32),
+        ],
+        in_specs=[VMEM] * 3,
+        out_specs=[VMEM] * 3,
+        name="finish_kernel",
+    )(ws, source_grad, target_grad)
+    return (target_grad, source_grad, weight_grad)
+
+
+def on_grid(target_rows, query_weight):
+    pairs = (lax.axis_size("sp"), lax.axis_size("tp")) == (2**3, 2**2)
+    heads = query_weight.shape[1] // HEAD_DIM
+    return pairs and heads % 2 == 0 and 2 * target_rows.shape[0] * lax.axis_size("tp") % 128 == 0
+
+
+def layer(*args):
+    return (grid_body if on_grid(args[0], args[3]) else body)(*args)
+
+
 def solution(mesh):
     in_specs = (
         P(("sp", "tp"), None),
@@ -574,4 +1011,4 @@
         P(("sp", "tp"), None),
     )
     out_specs = (P(("sp", "tp"), None), P(("sp", "tp"), None), P("sp", "tp"))
-    return jax.shard_map(body, mesh=mesh, in_specs=in_specs, out_specs=out_specs, check_vma=False)
+    return jax.shard_map(layer, mesh=mesh, in_specs=in_specs, out_specs=out_specs, check_vma=False)

time: 88.1 us -> 78.1 us (0.89)
  Pallas kernels: 81 us -> 77.3 us
  local copies, waits for them, and re-layouts: 3.44 us -> 0 us
  matrix products: 2.76 us -> 0 us
    pallas_call x1 -> x2, Pallas kernels: 81 us -> 77.3 us  [the longest x1 74.8 us: grid_body(): pl.pallas_call(functools.partial(grid_kernel, sp, tp, math.log(sblock * s...]
    unnamed x2 -> x0, local copies, waits for them, and re-layouts: 3.44 us -> none
    dot_general x1 -> x0, matrix products: 2.76 us -> none  [body(): lax.dot_general(cols_all.reshape(count, slice_width), flat_all.reshape(co...]
where the time goes in v1:
time: 78.1 us; the launch traced here: 77.9 us
  Pallas kernels  77.3 us (99%)
    pallas_call x1, Pallas kernels, grid_body(): pl.pallas_call(functools.partial(grid_kernel, sp, tp, math.log(sblock * s...  74.8 us
    pallas_call x1, Pallas kernels, grid_body(): pl.pallas_call(finish_kernel, out_shape=[jax.ShapeDtypeStruct((sw, width)...  2.44 us

profile of v1, /device:TPU:0, one launch (start us, length us, event | category | flops | bytes accessed | tf_op | source)
XLA Modules:
  0.0 77.9 jit_solution(11644928812810682385)
XLA Ops:
  0.6 74.8 %grid_kernel.1 = (bf16[2,2,256,256]{3,2,1,0:T(8,128)(2,1)}, f32[64,2048]{1,0:T(8,128)}, f32[16,2048]{1,0:T(8,128)}) custom-call(bf16[16,2048]{1,0:T(8,128)(2,1)} %raw.1, bf16[16,2048]{1,0:T(8,128)(2,1)} %to.1, bf16[64,2048]{1,0:T(8,128)(2,1)} %src.1, bf16[2048]{0:T(1024)(128)(2,1)} %gain.1, bf16[64,1024]{1,0:T(8,128)(2,1)} %saved.1, bf16[4,64]{1,0:T(4,128)(2,1)} %bitcast.1, ...), custom_call_target="tpu_custom_call" | custom-call | tf_op jit(solution)/shard_map/grid_kernel/pallas_call | solution.py:932
  75.5 2.4 %finish_kernel.1 = (f32[256,1024]{1,0:T(8,128)}, f32[64,2048]{1,0:T(8,128)}, f32[16,2048]{1,0:T(8,128)}) custom-call(bf16[2,2,256,256]{3,2,1,0:T(8,128)(2,1)} %get-tuple-element.9.ws, f32[64,2048]{1,0:T(8,128)} %get-tuple-element.10.src_in, f32[16,2048]{1,0:T(8,128)} %get-tuple-element.11.tgt_in), custom_call_target="tpu_custom_call" | custom-call | tf_op jit(solution)/shard_map/finish_kernel/pallas_call | solution.py:976

commit v2 on v0

--- a/solution.py
+++ b/solution.py
@@ -560,6 +560,536 @@
     return (target_grad, source_grad, weight_grad)
 
 
+class Net:
+    def __init__(self, send, recv):
+        self.sems, self.ids, self.started = (send, recv), {}, []
+
+    def _copy(self, name, src, dst, device):
+        n = self.ids.setdefault(name, len(self.ids))
+        return push(src, dst, self.sems[0].at[n], self.sems[1].at[n], device)
+
+    def go(self, name, src, dst, device):
+        copy = self._copy(name, src, dst, device)
+        copy.start()
+        self.started.append(copy)
+
+    def same(self, name, ref, device):
+        self.go(name, ref, ref, device)
+
+    def wait(self, name, landed, device):
+        self._copy(name, landed, landed, device).wait_recv()
+
+    def drain(self, count=None):
+        count = len(self.started) if count is None else count
+        for copy in self.started[:count]:
+            copy.wait_send()
+        self.started = self.started[count:]
+
+
+TRANSFERS = 176
+Y_FIRST = (False, False, True, True)
+
+
+def grid_kernel(
+    sp, tp, shift_base,
+    raw_h, to_h, src_h, gain_h, saved_h, offs_h, wq_h, wk_h, wv_h, wo_h,
+    ws_h, src_h_out, tgt_h_out,
+    raw, gain, saved, offs, ws, src_out, tgt_out,
+    tn_all, to_all, src_all, pieces, cols, q_st, g_st, sm_st, q_all, g_all, sm_all,
+    wq, wkv, wo, kv, p_s, d_s, part, xr, xs, ur, flat_all, fl, kv_sum, kvf,
+    sg, sd, ss, es, fs, fr, na, ng, ng1, ng2, ng3, wt,
+    wsem, osem, send, recv, *sems
+):
+    p = Place(sp, tp)
+    s, t, y, c, x = p.s, p.t, p.y, p.c, p.x
+    u, v = p.z // 2, p.z % 2
+    net = Net(send, recv)
+
+    def at(u, v, x):
+        return ((u * 2 + v) * 2 + x, t)
+
+    C, Y, V, X, U = p.partner, p.chip_y(1), at(u, 1 - v, x), at(u, v, 1 - x), at(1 - u, v, x)
+    ty, tc, tyc = (1 - y) * 2 + c, y * 2 + 1 - c, (1 - y) * 2 + 1 - c
+    others = [
+        (a, b, d, u + a - 2 * u * a, v + b - 2 * v * b, x + d - 2 * x * d)
+        for a in range(2) for b in range(2) for d in range(2) if a + b + d
+    ]
+    barrier = pltpu.get_barrier_semaphore()
+    friends = [C, Y] + [at(*o[3:]) for o in others]
+    for device in friends:
+        pl.semaphore_signal(barrier, inc=1, device_id=device, device_id_type=MESH)
+    rows, block, srows = raw.shape[0], saved.shape[0], src_h.shape[0]
+    model, width = wq.shape
+    heads = width // HEAD_DIM
+    hh, half = heads // 2, width // 2
+    sblock = srows * tp
+    sw = model // sp
+    quarters = len(Y_FIRST)
+    mq = model // quarters
+    scale = HEAD_DIM ** (-0.5)
+    mine = pl.ds(pl.multiple_of(v * half, half), half)
+    loads = [
+        pltpu.make_async_copy(h, w, wsem.at[i])
+        for i, (h, w) in enumerate(
+            (
+                (wq_h, wq), (wo_h, wo), (wk_h.at[:, mine], wkv.at[:, :half]), (wv_h.at[:, mine], wkv.at[:, half:]),
+                (raw_h, raw), (gain_h, gain), (src_h, src_all.at[v, t]), (to_h, to_all.at[t]),
+                (saved_h, saved), (offs_h, offs),
+            )
+        )
+    ]
+    for n in (4, 5, 6, 7, 0, 1, 8, 9, 2, 3):
+        loads[n].start()
+    loads[4].wait()
+    loads[5].wait()
+    raw_value, gain_value = raw[...].astype(F32), gain[...].astype(F32).reshape(1, model)
+    inverse = lax.rsqrt(jnp.mean(raw_value * raw_value, axis=1, keepdims=True) + EPSILON)
+    normed_value = (raw_value * inverse * gain_value).astype(BF)
+    tn_all[t] = normed_value
+    for a in range(2):
+        for b in range(2):
+            for k in range(2):
+                n = (2 * a + k) * 2 + b
+                pieces[a, b, :, k * sw : (k + 1) * sw] = normed_value[:, n * sw : (n + 1) * sw]
+    loads[6].wait()
+    loads[7].wait()
+    pl.semaphore_wait(barrier, len(friends))
+    A, B = pl.ds(0, srows // 2), pl.ds(srows // 2, srows // 2)
+
+    net.same("tnY", tn_all.at[t], Y)
+    net.same("sVB", src_all.at[v, t, B], V)
+    net.same("tnC", tn_all.at[t], C)
+    net.same("toY", to_all.at[t], Y)
+    net.same("toC", to_all.at[t], C)
+    net.same("sYA", src_all.at[v, t, A], Y)
+    net.same("sVA", src_all.at[v, t, A], V)
+    net.same("sYB", src_all.at[v, t, B], Y)
+    net.same("sC", src_all.at[v, t], C)
+    net.wait("tnY", tn_all.at[ty], Y)
+    net.same("tnF", tn_all.at[ty], C)
+    net.wait("toY", to_all.at[ty], Y)
+    net.same("toF", to_all.at[ty], C)
+    net.wait("tnC", tn_all.at[tc], C)
+    net.wait("tnF", tn_all.at[tyc], C)
+    loads[0].wait()
+    tn_b = tn_all[...].reshape(block, model)
+    for k in range(2):
+        for j in range(0, half, HEAD_DIM):
+            q_st[k, :, j : j + HEAD_DIM] = jnp.dot(
+                tn_b, wq[:, k * half + j : k * half + j + HEAD_DIM], preferred_element_type=F32
+            ).astype(BF)
+    net.go("qV", q_st.at[1 - v], q_all.at[u, x, v], V)
+    q_all[u, x, v] = q_st[v]
+    net.same("q0U", q_all.at[u, x, v], U)
+    net.same("q0X", q_all.at[u, x, v], X)
+    net.wait("sVB", src_all.at[1 - v, t, B], V)
+    net.same("fVB", src_all.at[1 - v, t, B], Y)
+    net.same("cVB", src_all.at[1 - v, t, B], C)
+    net.wait("toC", to_all.at[tc], C)
+    net.wait("toF", to_all.at[tyc], C)
+    loads[1].wait()
+    loads[8].wait()
+    loads[9].wait()
+    to_b = to_all[...].reshape(block, model)
+    products = []
+    for n in range(heads):
+        cut = slice(n * HEAD_DIM, (n + 1) * HEAD_DIM)
+        part_h = contract_last(to_b, wo[cut, :]).astype(BF)
+        g_st[n // hh, :, n % hh * HEAD_DIM : (n % hh + 1) * HEAD_DIM] = part_h
+        products.append(part_h.astype(F32) * saved[:, cut].astype(F32))
+    net.go("gV", g_st.at[1 - v], g_all.at[u, x, v], V)
+    g_all[u, x, v] = g_st[v]
+    net.same("g0U", g_all.at[u, x, v], U)
+    net.same("g0X", g_all.at[u, x, v], X)
+    lines, lanes = sm_st.shape[1], 2 * block
+    place = (
+        lax.broadcasted_iota(jnp.int32, (block, lanes), 1)
+        == lax.broadcasted_iota(jnp.int32, (block, lanes), 0) + v * block
+    ).astype(F32)
+    spread = jnp.dot(offs[...].astype(F32), place, precision=lax.Precision.HIGHEST, preferred_element_type=F32)
+    product = jnp.concatenate(products, axis=1)
+    line = lax.broadcasted_iota(jnp.int32, (2 * lines, width), 0)
+    head = lax.broadcasted_iota(jnp.int32, (2 * lines, width), 1) // HEAD_DIM
+    pick = (line == head // hh * lines + hh + head % hh).astype(BF)
+    deltas = 0.0
+    for term in range(3):
+        narrow = product.astype(BF)
+        product = product - narrow.astype(F32)
+        padded = jnp.concatenate(
+            [jnp.where(v == 0, narrow, jnp.zeros_like(narrow)), jnp.where(v == 1, narrow, jnp.zeros_like(narrow))],
+            axis=0,
+        )
+        deltas = deltas + contract_last(pick, padded)
+    line = lax.broadcasted_iota(jnp.int32, (lines, lanes), 0)
+    for k in range(2):
+        small = deltas[k * lines : (k + 1) * lines]
+        for h in range(hh):
+            n = k * hh + h
+            small = jnp.where(line == h, jnp.broadcast_to(spread[n : n + 1], small.shape), small)
+        sm_st[k] = small.astype(BF)
+    net.go("mV", sm_st.at[1 - v], sm_all.at[u, x, v], V)
+    sm_all[u, x, v] = sm_st[v]
+    net.same("m0U", sm_all.at[u, x, v], U)
+    net.same("m0X", sm_all.at[u, x, v], X)
+
+    net.wait("sYA", src_all.at[v, ty, A], Y)
+    net.same("cYA", src_all.at[v, ty, A], C)
+    net.wait("qV", q_all.at[u, x, 1 - v], V)
+    net.same("q1U", q_all.at[u, x, 1 - v], U)
+    net.same("q1X", q_all.at[u, x, 1 - v], X)
+    net.wait("sVA", src_all.at[1 - v, t, A], V)
+    net.same("fVA", src_all.at[1 - v, t, A], Y)
+    net.same("cVA", src_all.at[1 - v, t, A], C)
+    net.wait("gV", g_all.at[u, x, 1 - v], V)
+    net.same("g1U", g_all.at[u, x, 1 - v], U)
+    net.same("g1X", g_all.at[u, x, 1 - v], X)
+    net.wait("sYB", src_all.at[v, ty, B], Y)
+    net.same("cYB", src_all.at[v, ty, B], C)
+    net.wait("mV", sm_all.at[u, x, 1 - v], V)
+    net.same("m1U", sm_all.at[u, x, 1 - v], U)
+    net.same("m1X", sm_all.at[u, x, 1 - v], X)
+    def project(k, y):
+        count = 2 * srows
+        spot = pl.ds(pl.multiple_of(k * sblock + y * count, count), count)
+
+        @pl.loop(0, 2)
+        def _(j):
+            cut = pl.ds(pl.multiple_of(j * half, half), half)
+            value = src_all[k, pl.ds(2 * y, 2)].reshape(count, model)
+            kv[spot, cut] = jnp.dot(value, wkv[:, cut], preferred_element_type=F32).astype(BF)
+
+    net.wait("sC", src_all.at[v, tc], C)
+    loads[2].wait()
+    loads[3].wait()
+    project(v, y)
+    spot = (u * 2 + x) * 2 + v
+    for a, b, d, u2, v2, x2 in others:
+        net.go(f"p{a}{b}{d}", pieces.at[u2, x2], cols.at[spot, t], at(u2, v2, x2))
+    cols[spot, t] = pieces[u, x]
+    net.wait("q0U", q_all.at[1 - u, x, v], U)
+    net.same("q2X", q_all.at[1 - u, x, v], X)
+    net.wait("cVB", src_all.at[1 - v, tc, B], C)
+    net.wait("cVA", src_all.at[1 - v, tc, A], C)
+    project(1 - v, y)
+    net.wait("cYA", src_all.at[v, tyc, A], C)
+    net.wait("cYB", src_all.at[v, tyc, B], C)
+    net.wait("fVB", src_all.at[1 - v, ty, B], Y)
+    net.same("dVB", src_all.at[1 - v, ty, B], C)
+    net.wait("g0U", g_all.at[1 - u, x, v], U)
+    net.same("g2X", g_all.at[1 - u, x, v], X)
+    project(v, 1 - y)
+    net.wait("fVA", src_all.at[1 - v, ty, A], Y)
+    net.same("dVA", src_all.at[1 - v, ty, A], C)
+    net.wait("m0U", sm_all.at[1 - u, x, v], U)
+    net.same("m2X", sm_all.at[1 - u, x, v], X)
+    net.wait("q1U", q_all.at[1 - u, x, 1 - v], U)
+    net.same("q3X", q_all.at[1 - u, x, 1 - v], X)
+    net.wait("dVB", src_all.at[1 - v, tyc, B], C)
+    net.wait("dVA", src_all.at[1 - v, tyc, A], C)
+    project(1 - v, 1 - y)
+
+    def attend(w, after):
+        little = sm_all[w].astype(F32)
+        little = jnp.concatenate([little[0, 0] + little[0, 1], little[1, 0] + little[1, 1]], axis=1)
+        for h in range(hh):
+            cut = slice(h * HEAD_DIM, (h + 1) * HEAD_DIM)
+            q_h = q_all[w, :, :, :, cut].reshape(4 * block, HEAD_DIM)
+            g_h = g_all[w, :, :, :, cut].reshape(4 * block, HEAD_DIM)
+            prob = jnp.exp(contract_last(kv[:, cut], q_h) * scale - (shift_base + little[h : h + 1]))
+            grad = contract_last(kv[:, half + h * HEAD_DIM : half + (h + 1) * HEAD_DIM], g_h)
+            score = (prob * (grad - little[hh + h : hh + h + 1]) * scale).astype(BF)
+            p_s[h] = prob.astype(BF)
+            d_s[h] = score
+            term = lax.dot_general(score, kv[:, cut], (((0,), (0,)), ((), ())), preferred_element_type=F32)
+            part[w, :, h] = term.astype(BF).reshape(2, 2, block, HEAD_DIM)
+            after(h)
+
+    def source_terms(w):
+        for h in range(hh):
+            cut = slice(h * HEAD_DIM, (h + 1) * HEAD_DIM)
+            q_h = q_all[w, :, :, :, cut].reshape(4 * block, HEAD_DIM)
+            g_h = g_all[w, :, :, :, cut].reshape(4 * block, HEAD_DIM)
+            yield cut, jnp.dot(d_s[h], q_h, preferred_element_type=F32)
+            cut = slice(half + h * HEAD_DIM, half + (h + 1) * HEAD_DIM)
+            yield cut, jnp.dot(p_s[h], g_h, preferred_element_type=F32)
+
+    def send_near(h):
+        net.go(f"a{h}X", part.at[u, 1 - x, h], xr.at[0, h], X)
+
+    def send_far(h):
+        for k in range(2):
+            net.go(f"b{h}{k}X", part.at[1 - u, 1 - x, h, k], xr.at[1, h, k], X)
+
+    for n, k in ((0, v), (1, 1 - v)):
+        net.wait(f"q{n}X", q_all.at[u, 1 - x, k], X)
+        net.wait(f"m{n}X", sm_all.at[u, 1 - x, k], X)
+        net.wait(f"g{n}X", g_all.at[u, 1 - x, k], X)
+    attend(u, lambda h: None if h else send_near(h))
+    net.wait("g1U", g_all.at[1 - u, x, 1 - v], U)
+    net.same("g3X", g_all.at[1 - u, x, 1 - v], X)
+    net.wait("m1U", sm_all.at[1 - u, x, 1 - v], U)
+    net.same("m3X", sm_all.at[1 - u, x, 1 - v], X)
+    for h in range(1, hh):
+        send_near(h)
+    for cut, value in source_terms(u):
+        kv_sum[:, cut] = value
+
+    def near(h):
+        net.wait(f"a{h}X", xr.at[0, h], X)
+        xs[0, h] = (part[u, x, h].astype(F32) + xr[0, h].astype(F32)).astype(BF)
+        net.go(f"s{h}U", xs.at[0, h], ur.at[1, h], U)
+
+    near(0)
+    early = len(net.started)
+    for n, k in ((2, v), (3, 1 - v)):
+        net.wait(f"q{n}X", q_all.at[1 - u, 1 - x, k], X)
+        net.wait(f"m{n}X", sm_all.at[1 - u, 1 - x, k], X)
+        net.wait(f"g{n}X", g_all.at[1 - u, 1 - x, k], X)
+    attend(1 - u, send_far)
+    for h in range(1, hh):
+        near(h)
+    for cut, value in source_terms(1 - u):
+        kvf[:, cut] = (kv_sum[:, cut] + value).astype(BF)
+    for a, b, d, u2, v2, x2 in others:
+        net.wait(f"p{a}{b}{d}", cols.at[(u2 * 2 + x2) * 2 + v2, t], at(u2, v2, x2))
+    net.same("kY", cols.at[:, t], Y)
+    net.same("kC", cols.at[:, t], C)
+    stile = min(mq, 256)
+
+    def source(n):
+        for j in range(0, mq, stile):
+            value = contract_last(kvf[...], wkv[n * mq + j : n * mq + j + stile, :]).astype(BF)
+            sg[n, :, :, :, j : j + stile] = value.reshape(4, 2, srows, stile)
+        net.go(f"d{n}", sg.at[n, :, 1 - c], sd.at[n], C)
+
+    def source_sum(n):
+        net.wait(f"d{n}", sd.at[n], C)
+        for k in range(4):
+            ss[n, k] = (sg[n, k, c].astype(F32) + sd[n, k].astype(F32)).astype(BF)
+        first, keep = (Y, 2 * v + 1 - y) if Y_FIRST[n] else (V, 2 * (1 - v) + y)
+        net.go(f"e{n}1", ss.at[n, 2 * (1 - v) + 1 - y], es.at[n, 1], first)
+        net.go(f"e{n}0", ss.at[n, keep], es.at[n, 0], first)
+
+    def source_pass(n):
+        first, last = (Y, V) if Y_FIRST[n] else (V, Y)
+        keep = 2 * (1 - v) + y if Y_FIRST[n] else 2 * v + 1 - y
+        net.wait(f"e{n}1", es.at[n, 1], first)
+        fs[n] = (ss[n, keep].astype(F32) + es[n, 1].astype(F32)).astype(BF)
+        net.go(f"f{n}", fs.at[n], fr.at[n], last)
+
+    kept = []
+
+    def keep(ref, out):
+        copy = pltpu.make_async_copy(ref, out, osem.at[len(kept)])
+        copy.start()
+        kept.append(copy)
+
+    def source_end(n):
+        first, last = (Y, V) if Y_FIRST[n] else (V, Y)
+        net.wait(f"e{n}0", es.at[n, 0], first)
+        net.wait(f"f{n}", fr.at[n], last)
+        src_out[n] = ss[n, 2 * v + y].astype(F32) + es[n, 0].astype(F32) + fr[n].astype(F32)
+        keep(src_out.at[n], src_h_out.at[n])
+
+    def far(h):
+        for k in range(2):
+            net.wait(f"b{h}{k}X", xr.at[1, h, k], X)
+            xs[1, h, k] = (part[1 - u, x, h, k].astype(F32) + xr[1, h, k].astype(F32)).astype(BF)
+            net.go(f"z{h}{k}U", xs.at[1, h, k], ur.at[0, h, k], U)
+
+    def flat_far(h):
+        net.wait(f"s{h}U", ur.at[1, h], U)
+        flat_all[1 - u, x, h] = (xs[1, h].astype(F32) + ur[1, h].astype(F32)).astype(BF)
+        net.same(f"w{h}X", flat_all.at[1 - u, x, h], X)
+
+    def flat_near(h):
+        for k in range(2):
+            net.wait(f"z{h}{k}U", ur.at[0, h, k], U)
+            flat_all[u, x, h, k] = (xs[0, h, k].astype(F32) + ur[0, h, k].astype(F32)).astype(BF)
+            net.same(f"r{h}{k}X", flat_all.at[u, x, h, k], X)
+        net.go(f"n{h}V", flat_all.at[u, x, h, 1 - v], fl.at[v, h], V)
+        fl[v, h] = flat_all[u, x, h, v]
+
+    def weight(h):
+        for k in range(2):
+            net.wait(f"r{h}{k}X", flat_all.at[u, 1 - x, h, k], X)
+        net.wait(f"w{h}X", flat_all.at[1 - u, 1 - x, h], X)
+        flat_h = flat_all[:, :, h].reshape(sp * block, HEAD_DIM)
+        for k in range(2):
+            wt[h, k] = lax.dot_general(
+                cols[:, :, :, k * sw : (k + 1) * sw].reshape(sp * block, sw), flat_h,
+                (((0,), (0,)), ((), ())), preferred_element_type=F32,
+            ).astype(BF)
+        net.go(f"W{h}", wt.at[h, 1 - v], ws.at[v, h], V)
+        ws[v, h] = wt[h, v]
+        keep(ws.at[v, h], ws_h.at[v, h])
+
+    ntile = min(model, 256)
+
+    def normed_term(h):
+        net.wait(f"n{h}V", fl.at[1 - v, h], V)
+        for j in range(0, model, ntile):
+            columns = 0.0 if h == 0 else na[:, j : j + ntile]
+            for k in range(2):
+                n = (k * hh + h) * HEAD_DIM
+                columns = columns + contract_last(fl[k, h], wq[j : j + ntile, n : n + HEAD_DIM])
+            if h < hh - 1:
+                na[:, j : j + ntile] = columns
+            else:
+                ng[:, :, j : j + ntile] = columns.astype(BF).reshape(tp, rows, ntile)
+
+    source(0)
+    far(0)
+    source(1)
+    for h in range(1, hh):
+        far(h)
+    source_sum(0)
+    flat_far(0)
+    source(2)
+    for h in range(1, hh):
+        flat_far(h)
+    source_sum(1)
+    source(3)
+    source_sum(2)
+    net.wait("kY", cols.at[:, ty], Y)
+    net.same("kF", cols.at[:, ty], C)
+    net.drain(early)
+    flat_near(0)
+    source_sum(3)
+    source_pass(0)
+    net.wait("kC", cols.at[:, tc], C)
+    net.wait("kF", cols.at[:, tyc], C)
+    for h in range(1, hh):
+        flat_near(h)
+    source_pass(1)
+    weight(0)
+    source_pass(2)
+    normed_term(0)
+    source_end(0)
+    for h in range(1, hh):
+        weight(h)
+    late = len(net.started) - 6
+    for h in range(1, hh):
+        normed_term(h)
+    normed = PairScatter(p, lambda n: ng.at[n], ng1, ng2, ng3, *sems)
+    normed.start()
+    source_pass(3)
+    normed.middle()
+    source_end(1)
+    raw_value, gain_value = raw[...].astype(F32), gain[...].astype(F32).reshape(1, model)
+    inverse = lax.rsqrt(jnp.mean(raw_value * raw_value, axis=1, keepdims=True) + EPSILON)
+    source_end(2)
+    net.drain(late)
+    scaled = normed.finish() * gain_value
+    tgt_out[...] = inverse * scaled - raw_value * (inverse * inverse * inverse) * jnp.mean(
+        scaled * raw_value, axis=1, keepdims=True
+    )
+    keep(tgt_out, tgt_h_out)
+    source_end(3)
+    for h in range(hh):
+        net.wait(f"W{h}", ws.at[1 - v, h], V)
+        keep(ws.at[1 - v, h], ws_h.at[1 - v, h])
+    net.drain()
+    for copy in kept:
+        copy.wait()
+
+
+def finish_kernel(ws, src_in, tgt_in, weight_out, src_out, tgt_out):
+    parts, hh = ws.shape[0], ws.shape[1]
+    for k in range(parts):
+        for h in range(hh):
+            n = (k * hh + h) * HEAD_DIM
+            weight_out[:, n : n + HEAD_DIM] = ws[k, h].astype(F32)
+    quarters, mq = src_in.shape[0], src_in.shape[2]
+    for n in range(quarters):
+        src_out[:, n * mq : (n + 1) * mq] = src_in[n]
+    tgt_out[...] = tgt_in[...]
+
+
+def grid_body(
+    target_rows, source_rows, norm_gain, query_weight, key_weight, value_weight, output_weight,
+    saved_output, norm_offset, output_grad
+):
+    tp, sp = lax.axis_size("tp"), lax.axis_size("sp")
+    model, width = query_weight.shape
+    heads = width // HEAD_DIM
+    hh, half = heads // 2, width // 2
+    rows, srows = target_rows.shape[0], source_rows.shape[0]
+    block, sblock, sw = rows * tp, srows * tp, model // sp
+    Y = tp // 2
+    dma, vm = pltpu.SemaphoreType.DMA, pltpu.VMEM
+    whole = pl.BlockSpec(memory_space=pl.ANY)
+    quarters = len(Y_FIRST)
+    mq = model // quarters
+    ws, source_grad, target_grad = pl.pallas_call(
+        functools.partial(grid_kernel, sp, tp, math.log(sblock * sp)),
+        out_shape=[
+            jax.ShapeDtypeStruct((2, hh, sw, HEAD_DIM), BF),
+            jax.ShapeDtypeStruct((quarters, srows, mq), F32),
+            jax.ShapeDtypeStruct((rows, model), F32),
+        ],
+        in_specs=[whole] * 10,
+        out_specs=[whole] * 3,
+        scratch_shapes=[vm((rows, model), BF), vm((model,), BF), vm((block, width), BF), vm((heads, block), BF)]
+        + [vm((2, hh, sw, HEAD_DIM), BF), vm((quarters, srows, mq), F32), vm((rows, model), F32)]
+        + [vm((tp, rows, model), BF)] * 2
+        + [vm((2, tp, srows, model), BF)]
+        + [vm((2, 2, rows, 2 * sw), BF), vm((sp, tp, rows, 2 * sw), BF)]
+        + [vm((2, block, half), BF)] * 2
+        + [vm((2, 16, 2 * block), BF)]
+        + [vm((2, 2, 2, block, half), BF)] * 2
+        + [vm((2, 2, 2, 16, 2 * block), BF)]
+        + [vm((model, width), BF)] * 2
+        + [vm((width, model), BF)]
+        + [vm((2 * sblock, width), BF)]
+        + [vm((hh, 2 * sblock, 4 * block), BF)] * 2
+        + [vm((2, 2, hh, 2, block, HEAD_DIM), BF)]
+        + [vm((2, hh, 2, block, HEAD_DIM), BF)] * 3
+        + [vm((2, 2, hh, 2, block, HEAD_DIM), BF)]
+        + [vm((2, hh, block, HEAD_DIM), BF)]
+        + [vm((2 * sblock, width), F32), vm((2 * sblock, width), BF)]
+        + [vm((quarters, 4, 2, srows, mq), BF)]
+        + [vm((quarters, 4, srows, mq), BF)] * 2
+        + [vm((quarters, 2, srows, mq), BF)]
+        + [vm((quarters, srows, mq), BF)] * 2
+        + [vm((block, model), F32)]
+        + [vm((tp, rows, model), BF)]
+        + [vm((Y, rows, model), BF)] * 3
+        + [vm((hh, 2, sw, HEAD_DIM), BF)]
+        + [dma((10,)), dma((quarters + 2 * hh + 1,)), dma((TRANSFERS,)), dma((TRANSFERS,))]
+        + [dma((Y,))] * 4,
+        name="grid_kernel",
+        compiler_params=pltpu.CompilerParams(
+            collective_id=1, has_side_effects=True, vmem_limit_bytes=58 * 2**20
+        ),
+    )(
+        target_rows, output_grad, source_rows, norm_gain, saved_output, norm_offset.T,
+        query_weight, key_weight, value_weight, output_weight,
+    )
+    weight_grad, source_grad, target_grad = pl.pallas_call(
+        finish_kernel,
+        out_shape=[
+            jax.ShapeDtypeStruct((sw, width), F32),
+            jax.ShapeDtypeStruct((srows, model), F32),
+            jax.ShapeDtypeStruct((rows, model), F32),
+        ],
+        in_specs=[VMEM] * 3,
+        out_specs=[VMEM] * 3,
+        name="finish_kernel",
+    )(ws, source_grad, target_grad)
+    return (target_grad, source_grad, weight_grad)
+
+
+def on_grid(target_rows, query_weight):
+    pairs = (lax.axis_size("sp"), lax.axis_size("tp")) == (2**3, 2**2)
+    heads = query_weight.shape[1] // HEAD_DIM
+    return pairs and heads % 2 == 0 and 2 * target_rows.shape[0] * lax.axis_size("tp") % 128 == 0
+
+
+def layer(*args):
+    return (grid_body if on_grid(args[0], args[3]) else body)(*args)
+
+
 def solution(mesh):
     in_specs = (
         P(("sp", "tp"), None),
@@ -574,4 +1104,4 @@
         P(("sp", "tp"), None),
     )
     out_specs = (P(("sp", "tp"), None), P(("sp", "tp"), None), P("sp", "tp"))
-    return jax.shard_map(body, mesh=mesh, in_specs=in_specs, out_specs=out_specs, check_vma=False)
+    return jax.shard_map(layer, mesh=mesh, in_specs=in_specs, out_specs=out_specs, check_vma=False)

time: 88.1 us -> 63.5 us (0.72)
  Pallas kernels: 81 us -> 62.7 us
  local copies, waits for them, and re-layouts: 3.44 us -> 0 us
  matrix products: 2.76 us -> 0 us
    pallas_call x1 -> x2, Pallas kernels: 81 us -> 62.7 us  [the longest x1 60.2 us: grid_body(): pl.pallas_call(functools.partial(grid_kernel, sp, tp, math.log(sblock * s...]
    unnamed x2 -> x0, local copies, waits for them, and re-layouts: 3.44 us -> none
    dot_general x1 -> x0, matrix products: 2.76 us -> none  [body(): lax.dot_general(cols_all.reshape(count, slice_width), flat_all.reshape(co...]
where the time goes in v2:
time: 63.5 us; the launch traced here: 63.3 us
  Pallas kernels  62.7 us (99%)
  between operations  0.64 us (1%)
    pallas_call x1, Pallas kernels, grid_body(): pl.pallas_call(functools.partial(grid_kernel, sp, tp, math.log(sblock * s...  60.2 us
    pallas_call x1, Pallas kernels, grid_body(): pl.pallas_call(finish_kernel, out_shape=[jax.ShapeDtypeStruct((sw, width)...  2.44 us

profile of v2, /device:TPU:0, one launch (start us, length us, event | category | flops | bytes accessed | tf_op | source)
XLA Modules:
  0.0 63.3 jit_solution(12613134819812223091)
XLA Ops:
  0.6 60.2 %grid_kernel.1 = (bf16[2,2,256,256]{3,2,1,0:T(8,128)(2,1)}, f32[4,64,512]{2,1,0:T(8,128)}, f32[16,2048]{1,0:T(8,128)}) custom-call(bf16[16,2048]{1,0:T(8,128)(2,1)} %raw_h.1, bf16[16,2048]{1,0:T(8,128)(2,1)} %to_h.1, bf16[64,2048]{1,0:T(8,128)(2,1)} %src_h.1, bf16[2048]{0:T(1024)(128)(2,1)} %gain_h.1, bf16[64,1024]{1,0:T(8,128)(2,1)} %saved_h.1, ...), custom_call_target="tpu_custom_call" | custom-call | tf_op jit(solution)/shard_map/grid_kernel/pallas_call | solution.py:1024
  60.9 2.4 %finish_kernel.1 = (f32[256,1024]{1,0:T(8,128)}, f32[64,2048]{1,0:T(8,128)}, f32[16,2048]{1,0:T(8,128)}) custom-call(bf16[2,2,256,256]{3,2,1,0:T(8,128)(2,1)} %get-tuple-element.9.ws, f32[4,64,512]{2,1,0:T(8,128)} %get-tuple-element.10.src_in, f32[16,2048]{1,0:T(8,128)} %get-tuple-element.11.tgt_in), custom_call_target="tpu_custom_call" | custom-call | tf_op jit(solution)/shard_map/finish_kernel/pallas_call | solution.py:1069

commit v3 on v2

--- a/solution.py
+++ b/solution.py
@@ -562,16 +562,20 @@
 
 class Net:
     def __init__(self, send, recv):
-        self.sems, self.ids, self.started = (send, recv), {}, []
-
-    def _copy(self, name, src, dst, device):
+        self.send, self.recv, self.ids = send, recv, {}
+        self.free, self.started = list(range(send.shape[0])), []
+
+    def _copy(self, name, src, dst, device, slot=0):
         n = self.ids.setdefault(name, len(self.ids))
-        return push(src, dst, self.sems[0].at[n], self.sems[1].at[n], device)
+        return push(src, dst, self.send.at[slot], self.recv.at[n], device)
 
     def go(self, name, src, dst, device):
-        copy = self._copy(name, src, dst, device)
+        if not self.free:
+            self.drain(1)
+        slot = self.free.pop(0)
+        copy = self._copy(name, src, dst, device, slot)
         copy.start()
-        self.started.append(copy)
+        self.started.append((slot, copy))
 
     def same(self, name, ref, device):
         self.go(name, ref, ref, device)
@@ -581,13 +585,14 @@
 
     def drain(self, count=None):
         count = len(self.started) if count is None else count
-        for copy in self.started[:count]:
+        for slot, copy in self.started[:count]:
             copy.wait_send()
+            self.free.append(slot)
         self.started = self.started[count:]
 
 
-TRANSFERS = 176
-Y_FIRST = (False, False, True, True)
+SENDS = 28
+Y_FIRST = (False, True, True, True)
 
 
 def grid_kernel(
@@ -761,6 +766,8 @@
     net.wait("sC", src_all.at[v, tc], C)
     loads[2].wait()
     loads[3].wait()
+    net.wait("fVB", src_all.at[1 - v, ty, B], Y)
+    net.same("dVB", src_all.at[1 - v, ty, B], C)
     project(v, y)
     spot = (u * 2 + x) * 2 + v
     for a, b, d, u2, v2, x2 in others:
@@ -773,8 +780,6 @@
     project(1 - v, y)
     net.wait("cYA", src_all.at[v, tyc, A], C)
     net.wait("cYB", src_all.at[v, tyc, B], C)
-    net.wait("fVB", src_all.at[1 - v, ty, B], Y)
-    net.same("dVB", src_all.at[1 - v, ty, B], C)
     net.wait("g0U", g_all.at[1 - u, x, v], U)
     net.same("g2X", g_all.at[1 - u, x, v], X)
     project(v, 1 - y)
@@ -824,13 +829,11 @@
         net.wait(f"q{n}X", q_all.at[u, 1 - x, k], X)
         net.wait(f"m{n}X", sm_all.at[u, 1 - x, k], X)
         net.wait(f"g{n}X", g_all.at[u, 1 - x, k], X)
-    attend(u, lambda h: None if h else send_near(h))
     net.wait("g1U", g_all.at[1 - u, x, 1 - v], U)
     net.same("g3X", g_all.at[1 - u, x, 1 - v], X)
     net.wait("m1U", sm_all.at[1 - u, x, 1 - v], U)
     net.same("m3X", sm_all.at[1 - u, x, 1 - v], X)
-    for h in range(1, hh):
-        send_near(h)
+    attend(u, send_near)
     for cut, value in source_terms(u):
         kv_sum[:, cut] = value
 
@@ -839,17 +842,16 @@
         xs[0, h] = (part[u, x, h].astype(F32) + xr[0, h].astype(F32)).astype(BF)
         net.go(f"s{h}U", xs.at[0, h], ur.at[1, h], U)
 
-    near(0)
-    early = len(net.started)
     for n, k in ((2, v), (3, 1 - v)):
         net.wait(f"q{n}X", q_all.at[1 - u, 1 - x, k], X)
         net.wait(f"m{n}X", sm_all.at[1 - u, 1 - x, k], X)
         net.wait(f"g{n}X", g_all.at[1 - u, 1 - x, k], X)
     attend(1 - u, send_far)
+    near(0)
+    for cut, value in source_terms(1 - u):
+        kvf[:, cut] = (kv_sum[:, cut] + value).astype(BF)
     for h in range(1, hh):
         near(h)
-    for cut, value in source_terms(1 - u):
-        kvf[:, cut] = (kv_sum[:, cut] + value).astype(BF)
     for a, b, d, u2, v2, x2 in others:
         net.wait(f"p{a}{b}{d}", cols.at[(u2 * 2 + x2) * 2 + v2, t], at(u2, v2, x2))
     net.same("kY", cols.at[:, t], Y)
@@ -866,9 +868,11 @@
         net.wait(f"d{n}", sd.at[n], C)
         for k in range(4):
             ss[n, k] = (sg[n, k, c].astype(F32) + sd[n, k].astype(F32)).astype(BF)
-        first, keep = (Y, 2 * v + 1 - y) if Y_FIRST[n] else (V, 2 * (1 - v) + y)
-        net.go(f"e{n}1", ss.at[n, 2 * (1 - v) + 1 - y], es.at[n, 1], first)
-        net.go(f"e{n}0", ss.at[n, keep], es.at[n, 0], first)
+        net.go(f"e{n}1", ss.at[n, 2 * (1 - v) + 1 - y], es.at[n, 1], Y if Y_FIRST[n] else V)
+
+    def source_rest(n):
+        first, near = (Y, 2 * v + 1 - y) if Y_FIRST[n] else (V, 2 * (1 - v) + y)
+        net.go(f"e{n}0", ss.at[n, near], es.at[n, 0], first)
 
     def source_pass(n):
         first, last = (Y, V) if Y_FIRST[n] else (V, Y)
@@ -926,14 +930,15 @@
 
     ntile = min(model, 256)
 
-    def normed_term(h):
-        net.wait(f"n{h}V", fl.at[1 - v, h], V)
+    def normed_term(h, k, own):
+        if not own:
+            net.wait(f"n{h}V", fl.at[k, h], V)
+        cut = pl.ds(pl.multiple_of((k * hh + h) * HEAD_DIM, HEAD_DIM), HEAD_DIM)
         for j in range(0, model, ntile):
-            columns = 0.0 if h == 0 else na[:, j : j + ntile]
-            for k in range(2):
-                n = (k * hh + h) * HEAD_DIM
-                columns = columns + contract_last(fl[k, h], wq[j : j + ntile, n : n + HEAD_DIM])
-            if h < hh - 1:
+            columns = contract_last(fl[k, h], wq[j : j + ntile, cut])
+            if not own or h:
+                columns = columns + na[:, j : j + ntile]
+            if own or h < hh - 1:
                 na[:, j : j + ntile] = columns
             else:
                 ng[:, :, j : j + ntile] = columns.astype(BF).reshape(tp, rows, ntile)
@@ -943,43 +948,44 @@
     source(1)
     for h in range(1, hh):
         far(h)
+    source(2)
     source_sum(0)
-    flat_far(0)
-    source(2)
-    for h in range(1, hh):
-        flat_far(h)
+    source_rest(0)
+    source(3)
     source_sum(1)
-    source(3)
     source_sum(2)
     net.wait("kY", cols.at[:, ty], Y)
     net.same("kF", cols.at[:, ty], C)
-    net.drain(early)
+    source_sum(3)
+    for n in range(1, quarters):
+        source_rest(n)
+    for h in range(hh):
+        flat_far(h)
+    source_pass(1)
+    source_pass(2)
     flat_near(0)
-    source_sum(3)
-    source_pass(0)
+    normed_term(0, v, True)
     net.wait("kC", cols.at[:, tc], C)
     net.wait("kF", cols.at[:, tyc], C)
     for h in range(1, hh):
         flat_near(h)
-    source_pass(1)
+        normed_term(h, v, True)
+    source_pass(3)
     weight(0)
-    source_pass(2)
-    normed_term(0)
-    source_end(0)
+    source_pass(0)
+    normed_term(0, 1 - v, False)
     for h in range(1, hh):
         weight(h)
-    late = len(net.started) - 6
     for h in range(1, hh):
-        normed_term(h)
+        normed_term(h, 1 - v, False)
     normed = PairScatter(p, lambda n: ng.at[n], ng1, ng2, ng3, *sems)
     normed.start()
-    source_pass(3)
+    source_end(0)
+    source_end(1)
     normed.middle()
-    source_end(1)
+    source_end(2)
     raw_value, gain_value = raw[...].astype(F32), gain[...].astype(F32).reshape(1, model)
     inverse = lax.rsqrt(jnp.mean(raw_value * raw_value, axis=1, keepdims=True) + EPSILON)
-    source_end(2)
-    net.drain(late)
     scaled = normed.finish() * gain_value
     tgt_out[...] = inverse * scaled - raw_value * (inverse * inverse * inverse) * jnp.mean(
         scaled * raw_value, axis=1, keepdims=True
@@ -1056,7 +1062,7 @@
         + [vm((tp, rows, model), BF)]
         + [vm((Y, rows, model), BF)] * 3
         + [vm((hh, 2, sw, HEAD_DIM), BF)]
-        + [dma((10,)), dma((quarters + 2 * hh + 1,)), dma((TRANSFERS,)), dma((TRANSFERS,))]
+        + [dma((10,)), dma((quarters + 2 * hh + 1,)), dma((SENDS,)), dma((66 + 11 * hh,))]
         + [dma((Y,))] * 4,
         name="grid_kernel",
         compiler_params=pltpu.CompilerParams(

time: 63.5 us -> 59.4 us (0.935)
  Pallas kernels: 62.7 us -> 58.6 us
    pallas_call x1, Pallas kernels: 60.2 us -> 56.2 us  [grid_body(): pl.pallas_call(functools.partial(grid_kernel, sp, tp, math.log(sblock * s...]
where the time goes in v3:
time: 59.4 us; the launch traced here: 59.3 us
  Pallas kernels  58.6 us (99%)
  between operations  0.64 us (1%)
    pallas_call x1, Pallas kernels, grid_body(): pl.pallas_call(functools.partial(grid_kernel, sp, tp, math.log(sblock * s...  56.2 us
    pallas_call x1, Pallas kernels, grid_body(): pl.pallas_call(finish_kernel, out_shape=[jax.ShapeDtypeStruct((sw, width)...  2.44 us

profile of v3, /device:TPU:0, one launch (start us, length us, event | category | flops | bytes accessed | tf_op | source)
XLA Modules:
  0.0 59.3 jit_solution(18205804720892807122)
XLA Ops:
  0.6 56.2 %grid_kernel.1 = (bf16[2,2,256,256]{3,2,1,0:T(8,128)(2,1)}, f32[4,64,512]{2,1,0:T(8,128)}, f32[16,2048]{1,0:T(8,128)}) custom-call(bf16[16,2048]{1,0:T(8,128)(2,1)} %raw_h.1, bf16[16,2048]{1,0:T(8,128)(2,1)} %to_h.1, bf16[64,2048]{1,0:T(8,128)(2,1)} %src_h.1, bf16[2048]{0:T(1024)(128)(2,1)} %gain_h.1, bf16[64,1024]{1,0:T(8,128)(2,1)} %saved_h.1, ...), custom_call_target="tpu_custom_call" | custom-call | tf_op jit(solution)/shard_map/grid_kernel/pallas_call | solution.py:1030
  56.8 2.4 %finish_kernel.1 = (f32[256,1024]{1,0:T(8,128)}, f32[64,2048]{1,0:T(8,128)}, f32[16,2048]{1,0:T(8,128)}) custom-call(bf16[2,2,256,256]{3,2,1,0:T(8,128)(2,1)} %get-tuple-element.9.ws, f32[4,64,512]{2,1,0:T(8,128)} %get-tuple-element.10.src_in, f32[16,2048]{1,0:T(8,128)} %get-tuple-element.11.tgt_in), custom_call_target="tpu_custom_call" | custom-call | tf_op jit(solution)/shard_map/finish_kernel/pallas_call | solution.py:1075

commit v4 on v3

--- a/solution.py
+++ b/solution.py
@@ -591,7 +591,7 @@
         self.started = self.started[count:]
 
 
-SENDS = 28
+SENDS = 20
 Y_FIRST = (False, True, True, True)
 
 
@@ -599,11 +599,11 @@
     sp, tp, shift_base,
     raw_h, to_h, src_h, gain_h, saved_h, offs_h, wq_h, wk_h, wv_h, wo_h,
     ws_h, src_h_out, tgt_h_out,
-    raw, gain, saved, offs, ws, src_out, tgt_out,
+    raw, gain, saved, offs, src_out, tgt_out,
     tn_all, to_all, src_all, pieces, cols, q_st, g_st, sm_st, q_all, g_all, sm_all,
     wq, wkv, wo, kv, p_s, d_s, part, xr, xs, ur, flat_all, fl, kv_sum, kvf,
-    sg, sd, ss, es, fs, fr, na, ng, ng1, ng2, ng3, wt,
-    wsem, osem, send, recv, *sems
+    sg, sd, ss, es, fs, fr, na, ng, nr, wt,
+    wsem, osem, send, recv
 ):
     p = Place(sp, tp)
     s, t, y, c, x = p.s, p.t, p.y, p.c, p.x
@@ -620,7 +620,8 @@
         for a in range(2) for b in range(2) for d in range(2) if a + b + d
     ]
     barrier = pltpu.get_barrier_semaphore()
-    friends = [C, Y] + [at(*o[3:]) for o in others]
+    D = (s, tyc)
+    friends = [C, Y, D] + [at(*o[3:]) for o in others]
     for device in friends:
         pl.semaphore_signal(barrier, inc=1, device_id=device, device_id_type=MESH)
     rows, block, srows = raw.shape[0], saved.shape[0], src_h.shape[0]
@@ -924,9 +925,8 @@
                 cols[:, :, :, k * sw : (k + 1) * sw].reshape(sp * block, sw), flat_h,
                 (((0,), (0,)), ((), ())), preferred_element_type=F32,
             ).astype(BF)
-        net.go(f"W{h}", wt.at[h, 1 - v], ws.at[v, h], V)
-        ws[v, h] = wt[h, v]
-        keep(ws.at[v, h], ws_h.at[v, h])
+        net.go(f"W{h}", wt.at[h, 1 - v], ws_h.at[v, h], V)
+        keep(wt.at[h, v], ws_h.at[v, h])
 
     ntile = min(model, 256)
 
@@ -959,42 +959,42 @@
     source_sum(3)
     for n in range(1, quarters):
         source_rest(n)
+    source_pass(1)
     for h in range(hh):
         flat_far(h)
-    source_pass(1)
-    source_pass(2)
     flat_near(0)
+    source_pass(0)
     normed_term(0, v, True)
     net.wait("kC", cols.at[:, tc], C)
     net.wait("kF", cols.at[:, tyc], C)
     for h in range(1, hh):
         flat_near(h)
         normed_term(h, v, True)
+    source_pass(2)
+    weight(0)
     source_pass(3)
-    weight(0)
-    source_pass(0)
-    normed_term(0, 1 - v, False)
     for h in range(1, hh):
         weight(h)
-    for h in range(1, hh):
+    for h in range(hh):
         normed_term(h, 1 - v, False)
-    normed = PairScatter(p, lambda n: ng.at[n], ng1, ng2, ng3, *sems)
-    normed.start()
-    source_end(0)
-    source_end(1)
-    normed.middle()
-    source_end(2)
+    owners = ((tyc, D), (ty, Y), (tc, C))
+    for n, (k, device) in enumerate(owners):
+        net.go(f"o{n}", ng.at[k], nr.at[n], device)
+    for n in (0, 1, 2, 3):
+        source_end(n)
     raw_value, gain_value = raw[...].astype(F32), gain[...].astype(F32).reshape(1, model)
     inverse = lax.rsqrt(jnp.mean(raw_value * raw_value, axis=1, keepdims=True) + EPSILON)
-    scaled = normed.finish() * gain_value
+    scaled = ng[t].astype(F32)
+    for n, (_, device) in enumerate(owners):
+        net.wait(f"o{n}", nr.at[n], device)
+        scaled = scaled + nr[n].astype(F32)
+    scaled = scaled * gain_value
     tgt_out[...] = inverse * scaled - raw_value * (inverse * inverse * inverse) * jnp.mean(
         scaled * raw_value, axis=1, keepdims=True
     )
     keep(tgt_out, tgt_h_out)
-    source_end(3)
     for h in range(hh):
-        net.wait(f"W{h}", ws.at[1 - v, h], V)
-        keep(ws.at[1 - v, h], ws_h.at[1 - v, h])
+        net.wait(f"W{h}", ws_h.at[1 - v, h], V)
     net.drain()
     for copy in kept:
         copy.wait()
@@ -1022,7 +1022,6 @@
     hh, half = heads // 2, width // 2
     rows, srows = target_rows.shape[0], source_rows.shape[0]
     block, sblock, sw = rows * tp, srows * tp, model // sp
-    Y = tp // 2
     dma, vm = pltpu.SemaphoreType.DMA, pltpu.VMEM
     whole = pl.BlockSpec(memory_space=pl.ANY)
     quarters = len(Y_FIRST)
@@ -1037,7 +1036,7 @@
         in_specs=[whole] * 10,
         out_specs=[whole] * 3,
         scratch_shapes=[vm((rows, model), BF), vm((model,), BF), vm((block, width), BF), vm((heads, block), BF)]
-        + [vm((2, hh, sw, HEAD_DIM), BF), vm((quarters, srows, mq), F32), vm((rows, model), F32)]
+        + [vm((quarters, srows, mq), F32), vm((rows, model), F32)]
         + [vm((tp, rows, model), BF)] * 2
         + [vm((2, tp, srows, model), BF)]
         + [vm((2, 2, rows, 2 * sw), BF), vm((sp, tp, rows, 2 * sw), BF)]
@@ -1060,10 +1059,9 @@
         + [vm((quarters, srows, mq), BF)] * 2
         + [vm((block, model), F32)]
         + [vm((tp, rows, model), BF)]
-        + [vm((Y, rows, model), BF)] * 3
+        + [vm((3, rows, model), BF)]
         + [vm((hh, 2, sw, HEAD_DIM), BF)]
-        + [dma((10,)), dma((quarters + 2 * hh + 1,)), dma((SENDS,)), dma((66 + 11 * hh,))]
-        + [dma((Y,))] * 4,
+        + [dma((10,)), dma((quarters + hh + 1,)), dma((SENDS,)), dma((69 + 11 * hh,))],
         name="grid_kernel",
         compiler_params=pltpu.CompilerParams(
             collective_id=1, has_side_effects=True, vmem_limit_bytes=58 * 2**20

time: 59.4 us -> 59 us (level)
  no operation moved by 1% of the time
where the time goes in v4:
time: 59 us; the launch traced here: 58.8 us
  Pallas kernels  58.2 us (99%)
  between operations  0.64 us (1%)
    pallas_call x1, Pallas kernels, grid_body(): pl.pallas_call(functools.partial(grid_kernel, sp, tp, math.log(sblock * s...  55.7 us
    pallas_call x1, Pallas kernels, grid_body(): pl.pallas_call(finish_kernel, out_shape=[jax.ShapeDtypeStruct((sw, width)...  2.44 us

profile of v4, /device:TPU:0, one launch (start us, length us, event | category | flops | bytes accessed | tf_op | source)
XLA Modules:
  0.0 58.8 jit_solution(4822850937744573371)
XLA Ops:
  0.6 55.7 %grid_kernel.1 = (bf16[2,2,256,256]{3,2,1,0:T(8,128)(2,1)}, f32[4,64,512]{2,1,0:T(8,128)}, f32[16,2048]{1,0:T(8,128)}) custom-call(bf16[16,2048]{1,0:T(8,128)(2,1)} %raw_h.1, bf16[16,2048]{1,0:T(8,128)(2,1)} %to_h.1, bf16[64,2048]{1,0:T(8,128)(2,1)} %src_h.1, bf16[2048]{0:T(1024)(128)(2,1)} %gain_h.1, bf16[64,1024]{1,0:T(8,128)(2,1)} %saved_h.1, ...), custom_call_target="tpu_custom_call" | custom-call | tf_op jit(solution)/shard_map/grid_kernel/pallas_call | solution.py:1029
  56.4 2.4 %finish_kernel.1 = (f32[256,1024]{1,0:T(8,128)}, f32[64,2048]{1,0:T(8,128)}, f32[16,2048]{1,0:T(8,128)}) custom-call(bf16[2,2,256,256]{3,2,1,0:T(8,128)(2,1)} %get-tuple-element.9.ws, f32[4,64,512]{2,1,0:T(8,128)} %get-tuple-element.10.src_in, f32[16,2048]{1,0:T(8,128)} %get-tuple-element.11.tgt_in), custom_call_target="tpu_custom_call" | custom-call | tf_op jit(solution)/shard_map/finish_kernel/pallas_call | solution.py:1073

commit v5 on v4

--- a/solution.py
+++ b/solution.py
@@ -566,7 +566,7 @@
         self.free, self.started = list(range(send.shape[0])), []
 
     def _copy(self, name, src, dst, device, slot=0):
-        n = self.ids.setdefault(name, len(self.ids))
+        n = self.ids.setdefault(TOGETHER.get(name, name), len(self.ids))
         return push(src, dst, self.send.at[slot], self.recv.at[n], device)
 
     def go(self, name, src, dst, device):
@@ -591,7 +591,10 @@
         self.started = self.started[count:]
 
 
-SENDS = 20
+SENDS = 26
+TOGETHER = {f"p{n:03b}": "p" for n in range(8)}
+for first, second in (("q0X", "q1X"), ("g0X", "g1X"), ("m0X", "m1X"), ("q2X", "q3X"), ("g2X", "g3X"), ("m2X", "m3X"), ("cVB", "cVA"), ("dVB", "dVA"), ("cYA", "cYB")):
+    TOGETHER[second] = first
 Y_FIRST = (False, True, True, True)
 
 
@@ -776,11 +779,9 @@
     cols[spot, t] = pieces[u, x]
     net.wait("q0U", q_all.at[1 - u, x, v], U)
     net.same("q2X", q_all.at[1 - u, x, v], X)
-    net.wait("cVB", src_all.at[1 - v, tc, B], C)
-    net.wait("cVA", src_all.at[1 - v, tc, A], C)
+    net.wait("cVB", src_all.at[1 - v, tc], C)
     project(1 - v, y)
-    net.wait("cYA", src_all.at[v, tyc, A], C)
-    net.wait("cYB", src_all.at[v, tyc, B], C)
+    net.wait("cYA", src_all.at[v, tyc], C)
     net.wait("g0U", g_all.at[1 - u, x, v], U)
     net.same("g2X", g_all.at[1 - u, x, v], X)
     project(v, 1 - y)
@@ -790,8 +791,7 @@
     net.same("m2X", sm_all.at[1 - u, x, v], X)
     net.wait("q1U", q_all.at[1 - u, x, 1 - v], U)
     net.same("q3X", q_all.at[1 - u, x, 1 - v], X)
-    net.wait("dVB", src_all.at[1 - v, tyc, B], C)
-    net.wait("dVA", src_all.at[1 - v, tyc, A], C)
+    net.wait("dVB", src_all.at[1 - v, tyc], C)
     project(1 - v, 1 - y)
 
     def attend(w, after):
@@ -826,10 +826,9 @@
         for k in range(2):
             net.go(f"b{h}{k}X", part.at[1 - u, 1 - x, h, k], xr.at[1, h, k], X)
 
-    for n, k in ((0, v), (1, 1 - v)):
-        net.wait(f"q{n}X", q_all.at[u, 1 - x, k], X)
-        net.wait(f"m{n}X", sm_all.at[u, 1 - x, k], X)
-        net.wait(f"g{n}X", g_all.at[u, 1 - x, k], X)
+    net.wait("q0X", q_all.at[u, 1 - x], X)
+    net.wait("m0X", sm_all.at[u, 1 - x], X)
+    net.wait("g0X", g_all.at[u, 1 - x], X)
     net.wait("g1U", g_all.at[1 - u, x, 1 - v], U)
     net.same("g3X", g_all.at[1 - u, x, 1 - v], X)
     net.wait("m1U", sm_all.at[1 - u, x, 1 - v], U)
@@ -843,18 +842,16 @@
         xs[0, h] = (part[u, x, h].astype(F32) + xr[0, h].astype(F32)).astype(BF)
         net.go(f"s{h}U", xs.at[0, h], ur.at[1, h], U)
 
-    for n, k in ((2, v), (3, 1 - v)):
-        net.wait(f"q{n}X", q_all.at[1 - u, 1 - x, k], X)
-        net.wait(f"m{n}X", sm_all.at[1 - u, 1 - x, k], X)
-        net.wait(f"g{n}X", g_all.at[1 - u, 1 - x, k], X)
+    net.wait("q2X", q_all.at[1 - u, 1 - x], X)
+    net.wait("m2X", sm_all.at[1 - u, 1 - x], X)
+    net.wait("g2X", g_all.at[1 - u, 1 - x], X)
     attend(1 - u, send_far)
     near(0)
     for cut, value in source_terms(1 - u):
         kvf[:, cut] = (kv_sum[:, cut] + value).astype(BF)
     for h in range(1, hh):
         near(h)
-    for a, b, d, u2, v2, x2 in others:
-        net.wait(f"p{a}{b}{d}", cols.at[(u2 * 2 + x2) * 2 + v2, t], at(u2, v2, x2))
+    net.wait("p", cols.at[: len(others), t], V)
     net.same("kY", cols.at[:, t], Y)
     net.same("kC", cols.at[:, t], C)
     stile = min(mq, 256)
@@ -1061,7 +1058,7 @@
         + [vm((tp, rows, model), BF)]
         + [vm((3, rows, model), BF)]
         + [vm((hh, 2, sw, HEAD_DIM), BF)]
-        + [dma((10,)), dma((quarters + hh + 1,)), dma((SENDS,)), dma((69 + 11 * hh,))],
+        + [dma((10,)), dma((quarters + hh + 1,)), dma((SENDS,)), dma((54 + 11 * hh,))],
         name="grid_kernel",
         compiler_params=pltpu.CompilerParams(
             collective_id=1, has_side_effects=True, vmem_limit_bytes=58 * 2**20

time: 59 us -> 58.7 us (level)
  no operation moved by 1% of the time
where the time goes in v5:
time: 58.7 us; the launch traced here: 58.6 us
  Pallas kernels  57.9 us (99%)
  between operations  0.64 us (1%)
    pallas_call x1, Pallas kernels, grid_body(): pl.pallas_call(functools.partial(grid_kernel, sp, tp, math.log(sblock * s...  55.5 us
    pallas_call x1, Pallas kernels, grid_body(): pl.pallas_call(finish_kernel, out_shape=[jax.ShapeDtypeStruct((sw, width)...  2.44 us

profile of v5, /device:TPU:0, one launch (start us, length us, event | category | flops | bytes accessed | tf_op | source)
XLA Modules:
  0.0 58.6 jit_solution(17011892048383988950)
XLA Ops:
  0.6 55.5 %grid_kernel.1 = (bf16[2,2,256,256]{3,2,1,0:T(8,128)(2,1)}, f32[4,64,512]{2,1,0:T(8,128)}, f32[16,2048]{1,0:T(8,128)}) custom-call(bf16[16,2048]{1,0:T(8,128)(2,1)} %raw_h.1, bf16[16,2048]{1,0:T(8,128)(2,1)} %to_h.1, bf16[64,2048]{1,0:T(8,128)(2,1)} %src_h.1, bf16[2048]{0:T(1024)(128)(2,1)} %gain_h.1, bf16[64,1024]{1,0:T(8,128)(2,1)} %saved_h.1, ...), custom_call_target="tpu_custom_call" | custom-call | tf_op jit(solution)/shard_map/grid_kernel/pallas_call | solution.py:1026
  56.1 2.4 %finish_kernel.1 = (f32[256,1024]{1,0:T(8,128)}, f32[64,2048]{1,0:T(8,128)}, f32[16,2048]{1,0:T(8,128)}) custom-call(bf16[2,2,256,256]{3,2,1,0:T(8,128)(2,1)} %get-tuple-element.9.ws, f32[4,64,512]{2,1,0:T(8,128)} %get-tuple-element.10.src_in, f32[16,2048]{1,0:T(8,128)} %get-tuple-element.11.tgt_in), custom_call_target="tpu_custom_call" | custom-call | tf_op jit(solution)/shard_map/finish_kernel/pallas_call | solution.py:1070
